TPU v7x, 256 devices: a whole 4x4x8 slice. The times are simulated.
256 devices in a mesh: kv: 32 (over z, x), tp: 8 (over y, core).
Axes of the slice: x: 4, y: 4, z: 8, core: 2. Of those that a mesh axis runs over, the one named last changes fastest.
Arguments:
- stream: bfloat16 [512, 4096], P(None, ('kv', 'tp')), may hold values from -20 to 20
- ssm_state: float32 [512, 64, 64, 128], P('kv', 'tp'), may hold values from -1.8 to 1.8
- conv_state: bfloat16 [512, 3, 8, 768], P('kv', None, 'tp'), may hold values from -6 to 6
- first_gain: float32 [4096], P(('kv', 'tp')), may hold values from 0.1 to 1.9
- first_gate: bfloat16 [4096, 11264], P('kv', 'tp'), may hold values from -0.09375 to 0.09375
- first_up: bfloat16 [4096, 11264], P('kv', 'tp'), may hold values from -0.09375 to 0.09375
- first_down: bfloat16 [11264, 4096], P('tp', 'kv'), may hold values from -0.0546875 to 0.0546875
- mix_gain: float32 [4096], P(('kv', 'tp')), may hold values from 0.1 to 1.9
- gate_in: bfloat16 [4096, 4096], P('kv', 'tp'), may hold values from -0.09375 to 0.09375
- value_in: bfloat16 [4096, 4096], P('kv', 'tp'), may hold values from -0.09375 to 0.09375
- write_in: bfloat16 [4096, 1024], P('kv', 'tp'), may hold values from -0.09375 to 0.09375
- read_in: bfloat16 [4096, 1024], P('kv', 'tp'), may hold values from -0.09375 to 0.09375
- step_in: bfloat16 [4096, 64], P('kv', 'tp'), may hold values from -0.09375 to 0.09375
- conv_weight: float32 [4, 8, 768], P(None, 'tp'), may hold values from -3 to 3
- step_bias: float32 [64], P('tp'), may hold values from -3 to 0.5
- log_decay_rate: float32 [64], P('tp'), may hold values from -1 to 2.5
- group_gain: float32 [4096], P('tp'), may hold values from 0.1 to 1.9
- out_weight: bfloat16 [4096, 4096], P('tp', 'kv'), may hold values from -0.09375 to 0.09375
- last_norm_gain: float32 [4096], P(('kv', 'tp')), may hold values from 0.1 to 1.9
- second_gate: bfloat16 [4096, 11264], P('kv', 'tp'), may hold values from -0.09375 to 0.09375
- second_up: bfloat16 [4096, 11264], P('kv', 'tp'), may hold values from -0.09375 to 0.09375
- second_down: bfloat16 [11264, 4096], P('tp', 'kv'), may hold values from -0.109375 to 0.109375
Outputs:
- next_stream: bfloat16 [512, 4096], P(None, ('kv', 'tp'))
- ssm_next: float32 [512, 64, 64, 128], P('kv', 'tp')
- conv_next: bfloat16 [512, 3, 8, 768], P('kv', None, 'tp')
All inputs are finite; a program needn't handle non-finite values.
Results may differ from a plain program's by a relative error of at most 0.015.
Values may be sent and summed in bfloat16 or wider, within the bound.
A program may use at most 64 MiB of HBM per device.

v0:
```python
import jax
import jax.numpy as jnp
from jax import lax
from jax.sharding import Mesh
from jax.sharding import PartitionSpec as P

KV = ("kv_0", "kv_1")
KV_TP = ("kv_0", "kv_1", "tp")


norm_epsilon = 1e-06


def joined_along(tiles, dim):
    shape = list(tiles.shape[1:])
    shape[dim] *= tiles.shape[0]
    return jnp.moveaxis(tiles, 0, dim).reshape(shape)


def copy_for_each(array, axis):
    copies = jnp.broadcast_to(array, (lax.axis_size(axis), *array.shape))
    return lax.all_to_all(copies, axis, split_axis=0, concat_axis=0, tiled=True)


def gather_directly(array, axis, dim):
    return joined_along(copy_for_each(array, axis), dim)


def split_up(array, dim, length):
    before, after = (array.shape[:dim], array.shape[dim + 1 :])
    return jnp.moveaxis(array.reshape(*before, length, -1, *after), dim, 0)


def sum_at_owner(array, axis, dim):
    tiles = split_up(array, dim, lax.axis_size(axis))
    arrived = lax.all_to_all(tiles, axis, split_axis=0, concat_axis=0, tiled=True)
    return arrived.astype(jnp.float32).sum(axis=0)


def summed_rows(array, axes, dim):
    for axis in axes:
        array = lax.psum_scatter(array, axis, scatter_dimension=dim, tiled=True)
    return array


def gathered_by_axis(array, axes, dim):
    result = array
    for number in range(len(axes) - 1, -1, -1):
        result = lax.all_gather(result, axes[number], axis=dim, tiled=True)
    return result


def side_by_side(arrays, axis, dim, along):
    both = jnp.concatenate(arrays, axis=along)
    result, at, gathered = (lax.psum_scatter(both, axis, scatter_dimension=dim, tiled=True), 0, [])
    for a in arrays:
        gathered.append(lax.slice_in_dim(result, at, at + a.shape[along], axis=along))
        at += a.shape[along]
    return tuple(gathered)


def row_factor(total_squares, width):
    return lax.rsqrt(total_squares / width + norm_epsilon)[:, None]


def normed_rows(stream, gain):
    values = stream.astype(jnp.float32)
    scaled = (values * gain[None]).astype(jnp.bfloat16)
    squares = jnp.sum(values * values, axis=1)
    gathered, square_cols = (
        gather_directly(scaled, "tp", 1),
        gather_directly(squares[:, None].astype(jnp.bfloat16), "tp", 1).astype(jnp.float32),
    )
    return (gathered, jnp.sum(square_cols, axis=1))


def finish(stream, terms, weight_matrix):
    branch_output = sum_at_owner(terms.astype(jnp.bfloat16), "tp", 1)
    return (stream.astype(jnp.float32) + weight_matrix * branch_output).astype(jnp.bfloat16)


def channel_mixer(stream, gain, gate_weight, up_weight, down_weight):
    width = stream.shape[1] * lax.axis_size(KV) * lax.axis_size("tp")
    gathered, squares = normed_rows(stream, gain)
    gate_part = jnp.dot(gathered, gate_weight, preferred_element_type=jnp.float32)
    up_part = jnp.dot(gathered, up_weight, preferred_element_type=jnp.float32)
    gate_sum, up_sum, total = (
        summed_rows(gate_part, KV, 0),
        summed_rows(up_part, KV, 0),
        summed_rows(squares, KV, 0),
    )
    factor = row_factor(total, width)
    hidden = (jax.nn.silu(gate_sum * factor) * (up_sum * factor)).astype(jnp.bfloat16)
    terms = jnp.dot(
        gathered_by_axis(hidden, KV, 0), down_weight, preferred_element_type=jnp.float32
    )
    return finish(stream, terms, 0.5)


def token_mixer(
    stream,
    ssm_state,
    conv_state,
    gain,
    gate_in,
    value_in,
    write_in,
    read_in,
    step_in,
    conv_weight,
    step_bias,
    log_decay_rate,
    group_gain,
    out_weight,
):
    width_all = stream.shape[1] * lax.axis_size(KV) * lax.axis_size("tp")
    gathered, squares = normed_rows(stream, gain)
    gate_part = jnp.dot(gathered, gate_in, preferred_element_type=jnp.float32)
    value_part = jnp.dot(gathered, value_in, preferred_element_type=jnp.float32)
    write_part = jnp.dot(gathered, write_in, preferred_element_type=jnp.float32)
    read_part = jnp.dot(gathered, read_in, preferred_element_type=jnp.float32)
    step_part = jnp.dot(gathered, step_in, preferred_element_type=jnp.float32)
    count = stream.shape[0] // lax.axis_size(KV)
    gate_sum, value_sum, write_sum, read_sum, step_sum, total = (
        *side_by_side((gate_part, value_part, write_part, read_part, step_part), KV, 0, 1),
        lax.psum_scatter(squares, KV, scatter_dimension=0, tiled=True),
    )
    factor = row_factor(total, width_all)
    gate = (gate_sum * factor).astype(jnp.bfloat16)
    values = (value_sum * factor).astype(jnp.bfloat16)
    writes = (write_sum * factor).astype(jnp.bfloat16)
    reads = (read_sum * factor).astype(jnp.bfloat16)
    steps = (step_sum * factor).astype(jnp.bfloat16)
    groups = conv_weight.shape[1]
    state_size = write_in.shape[1] // groups
    heads = step_in.shape[1]
    head_size = value_in.shape[1] // heads
    per_group = heads // groups
    width = per_group * head_size
    fresh = jnp.concatenate(
        [
            values.reshape(count, groups, width),
            writes.reshape(count, groups, state_size),
            reads.reshape(count, groups, state_size),
        ],
        axis=2,
    )
    window = jnp.concatenate([conv_state, fresh[:, None]], axis=1)
    activated = jax.nn.silu(jnp.sum(window.astype(jnp.float32) * conv_weight[None], axis=1))
    inputs = activated[:, :, :width].reshape(count, groups, per_group, head_size)
    write_vec = activated[:, :, width : width + state_size]
    read_vec = activated[:, :, width + state_size :]
    step_size = jax.nn.softplus(steps.astype(jnp.float32) + step_bias[None])
    decay = jnp.exp(-step_size * jnp.exp(log_decay_rate)[None])
    step_size = step_size.reshape(count, groups, per_group)
    decay = decay.reshape(count, groups, per_group)
    carried = ssm_state.reshape(count, groups, per_group, head_size, state_size)
    updated = (
        carried * decay[:, :, :, None, None]
        + (step_size[:, :, :, None] * inputs)[..., None] * write_vec[:, :, None, None, :]
    )
    readout = jnp.einsum("bghpn,bgn->bghp", updated, read_vec).reshape(count, groups, width)
    gated = readout * jax.nn.silu(gate.astype(jnp.float32)).reshape(count, groups, width)
    normed = gated * lax.rsqrt(jnp.mean(gated * gated, axis=2, keepdims=True) + norm_epsilon)
    mixed = (
        (normed * group_gain.reshape(groups, width)[None])
        .astype(jnp.bfloat16)
        .reshape(count, groups * width)
    )
    terms = jnp.dot(gather_directly(mixed, KV, 0), out_weight, preferred_element_type=jnp.float32)
    after = finish(stream, terms, 1.0)
    return (after, updated.reshape(ssm_state.shape), window[:, 1:])


def on_device(
    stream,
    ssm_state,
    conv_state,
    first_gain,
    first_gate,
    first_up,
    first_down,
    mix_gain,
    gate_in,
    value_in,
    write_in,
    read_in,
    step_in,
    conv_weight,
    step_bias,
    log_decay_rate,
    group_gain,
    out_weight,
    last_norm_gain,
    second_gate,
    second_up,
    second_down,
):
    after_first = channel_mixer(stream, first_gain, first_gate, first_up, first_down)
    after_mix, ssm_next, conv_next = token_mixer(
        after_first,
        ssm_state,
        conv_state,
        mix_gain,
        gate_in,
        value_in,
        write_in,
        read_in,
        step_in,
        conv_weight,
        step_bias,
        log_decay_rate,
        group_gain,
        out_weight,
    )
    next_stream = channel_mixer(after_mix, last_norm_gain, second_gate, second_up, second_down)
    return (next_stream, ssm_next, conv_next)


def solution(mesh):
    finer = Mesh(mesh.devices.reshape(8, 4, mesh.shape["tp"]), ("kv_0", "kv_1", "tp"))
    placed = (
        P(None, KV_TP),
        P(KV, "tp", None, None),
        P(KV, None, "tp", None),
        P(KV_TP),
        P(KV, "tp"),
        P(KV, "tp"),
        P("tp", KV),
        P(KV_TP),
        P(KV, "tp"),
        P(KV, "tp"),
        P(KV, "tp"),
        P(KV, "tp"),
        P(KV, "tp"),
        P(None, "tp", None),
        P("tp"),
        P("tp"),
        P("tp"),
        P("tp", KV),
        P(KV_TP),
        P(KV, "tp"),
        P(KV, "tp"),
        P("tp", KV),
    )
    return jax.shard_map(
        on_device,
        mesh=finer,
        in_specs=placed,
        out_specs=(P(None, KV_TP), P(KV, "tp", None, None), P(KV, None, "tp", None)),
        check_vma=False,
    )
```

profile of v0, /device:TPU:1, one launch (start us, length us, event | category | flops | bytes accessed | tf_op | source)
XLA Modules:
  0.0 727.3 jit_solution(373540209757433886)
XLA Ops:
  7.2 0.8 fusion.9
  8.1 11.0 %all_to_all.50 = bf16[8,512,16]{1,2,0:T(8,128)(2,1)S(1)} all-to-all(bf16[8,512,16]{1,2,0:T(8,128)(2,1)S(1)} %broadcast_in_dim.14), channel_id=1, replica_groups=mesh['kv_0'=8,'kv_1'=4,'tp'=8] {'tp'}, dimensions={0} | all-to-all | bytes 262144 | tf_op jit(solution)/shard_map/all_to_all | solution.py:22
  19.1 2.1 fusion.33
  21.3 2.1 fusion.34
  23.6 39.9 %reduce-scatter.12.cloned.1.call-done = f32[64,1408]{1,0:T(8,128)} async-done(((f32[512,1408]{1,0:T(8,128)}), f32[64,1408]{1,0:T(8,128)}) %reduce-scatter.12.cloned.1.call-update) | async-done | bytes 360464 | tf_op jit(solution)/shard_map/reduce_scatter | solution.py:42
  63.5 48.5 %reduce-scatter.16.cloned.1.call-done = f32[64,1408]{1,0:T(8,128)} async-done(((f32[512,1408]{1,0:T(8,128)}), f32[64,1408]{1,0:T(8,128)}) %reduce-scatter.16.cloned.1.call-update) | async-done | bytes 360464 | tf_op jit(solution)/shard_map/reduce_scatter | solution.py:42
  112.0 0.5 broadcast.109
  112.5 0.7 reduce.9
  113.2 0.6 reshape.209
  113.9 8.9 %all-to-all-start.1 = ((bf16[8,2,256]{2,1,0:T(2,128)(2,1)}), bf16[8,2,256]{2,1,0:T(2,128)(2,1)S(1)}, u32[]{:S(2)}, u32[]{:S(2)}) async-start(bf16[8,2,256]{2,1,0:T(2,128)(2,1)} %reshape.209), calls=%async_computation.3 | async-start | bytes 16384 | tf_op jit(solution)/shard_map/all_to_all | solution.py:22
  122.8 0.6 dynamic-slice
  123.3 0.6 dynamic-slice.2
  125.3 2.1 all-to-all-done.1
  127.4 12.1 %all-reduce = f32[512]{0:T(512)S(1)} all-reduce(f32[512]{0:T(512)S(1)} %convert_reduce_fusion.5), channel_id=4, replica_groups=mesh['kv_0'=8,'kv_1'=4,'tp'=8] {'kv_0'}, use_global_device_ids=true, to_apply=%region_4.0.clone | all-reduce | flops 512 | bytes 4096
  139.6 9.4 %all-reduce.1 = f32[64]{0:T(128)S(1)} all-reduce(f32[64]{0:T(128)S(1)} %dynamic-slice.1), channel_id=5, replica_groups=mesh['kv_0'=8,'kv_1'=4,'tp'=8] {'kv_1'}, use_global_device_ids=true, to_apply=%region_5.0.clone | all-reduce | flops 64 | bytes 512
  149.1 16.0 %reduce-scatter.18.cloned.1.call-done = f32[16,1408]{1,0:T(8,128)} async-done(((f32[64,1408]{1,0:T(8,128)}), f32[16,1408]{1,0:T(8,128)}) %reduce-scatter.18.cloned.1.call-update) | async-done | bytes 90128 | tf_op jit(solution)/shard_map/reduce_scatter | solution.py:42
  165.1 1.0 multiply_convert_fusion.1
  166.1 10.5 %all_gather.12 = bf16[64,1408]{1,0:T(8,128)(2,1)} all-gather(bf16[16,1408]{1,0:T(8,128)(2,1)S(1)} %multiply_convert_fusion.1), channel_id=1, replica_groups=mesh['kv_0'=8,'kv_1'=4,'tp'=8] {'kv_1'}, dimensions={0}, use_global_device_ids=true | all-gather | bytes 225280 | tf_op jit(solution)/shard_map/all_gather | solution.py:49
  176.7 39.7 %all-gather.3.cloned.1.call-done = bf16[512,1408]{1,0:T(8,128)(2,1)} async-done(((bf16[64,1408]{1,0:T(8,128)(2,1)}), bf16[512,1408]{1,0:T(8,128)(2,1)}) %all-gather.3.cloned.1.call-update) | async-done | bytes 1441808 | tf_op jit(solution)/shard_map/all_gather | solution.py:49
  216.4 2.0 convolution_convert_fusion.2
  218.4 14.3 %all_to_all.51 = bf16[8,512,16]{1,2,0:T(8,128)(2,1)S(1)} all-to-all(bf16[8,512,16]{1,2,0:T(8,128)(2,1)S(1)} %bitcast.105), channel_id=1, replica_groups=mesh['kv_0'=8,'kv_1'=4,'tp'=8] {'tp'}, dimensions={0} | all-to-all | bytes 262144 | tf_op jit(solution)/shard_map/all_to_all | solution.py:36
  232.8 8.5 %all_to_all.52 = bf16[8,512,16]{1,2,0:T(8,128)(2,1)S(1)} all-to-all(bf16[8,512,16]{1,2,0:T(8,128)(2,1)S(1)} %broadcast_in_dim.16), channel_id=1, replica_groups=mesh['kv_0'=8,'kv_1'=4,'tp'=8] {'tp'}, dimensions={0} | all-to-all | bytes 262144 | tf_op jit(solution)/shard_map/all_to_all | solution.py:22
  241.3 0.3 convolution_dynamic-update-slice_fusion.1
  241.7 0.3 convolution_dynamic-update-slice_fusion
  242.0 0.2 convolution_dynamic-update-slice_fusion.3
  242.3 0.2 convolution_dynamic-update-slice_fusion.2
  242.5 0.1 convolution_dynamic-update-slice_fusion.4
  242.7 2.2 copy.50
  244.9 0.7 reduce.10
  245.7 0.6 reshape.211
  246.3 4.1 all-to-all-start.4
  250.4 0.6 dynamic-slice.4
  251.6 3.4 all-to-all-done.4
  255.1 59.3 %all-reduce.2 = f32[512]{0:T(512)S(1)} all-reduce(f32[512]{0:T(512)S(1)} %convert_reduce_fusion.4), channel_id=9, replica_groups=mesh['kv_0'=8,'kv_1'=4,'tp'=8] {'kv_0','kv_1'}, use_global_device_ids=true, to_apply=%region_12.13.clone | all-reduce | flops 512 | bytes 4096
  314.4 143.0 %reduce-scatter.28.cloned.1.call-done = f32[16,1288]{1,0:T(8,128)} async-done(((f32[512,1288]{1,0:T(8,128)}), f32[16,1288]{1,0:T(8,128)}) %reduce-scatter.28.cloned.1.call-update) | async-done | bytes 82448 | tf_op jit(solution)/shard_map/reduce_scatter | solution.py:55
  457.4 0.7 fusion.31
  458.1 0.1 copy.54
  458.5 0.9 fusion.21
  459.5 0.7 slice.36
  460.6 3.1 multiply_add_fusion
  463.7 2.0 copy-done.1
  465.7 1.7 fusion.35
  467.5 1.0 multiply_reduce_fusion.1
  468.7 19.0 %all_to_all.53 = bf16[32,16,512]{2,1,0:T(8,128)(2,1)S(1)} all-to-all(bf16[32,16,512]{2,1,0:T(8,128)(2,1)S(1)} %broadcast_in_dim.18), channel_id=1, replica_groups=mesh['kv_0'=8,'kv_1'=4,'tp'=8] {'kv_0','kv_1'}, dimensions={0} | all-to-all | bytes 1048576 | tf_op jit(solution)/shard_map/all_to_all | solution.py:22
  487.7 0.3 convolution_convert_fusion
  488.0 16.5 %all_to_all.54 = bf16[8,512,16]{1,2,0:T(8,128)(2,1)S(1)} all-to-all(bf16[8,512,16]{1,2,0:T(8,128)(2,1)S(1)} %bitcast.104), channel_id=1, replica_groups=mesh['kv_0'=8,'kv_1'=4,'tp'=8] {'tp'}, dimensions={0} | all-to-all | bytes 262144 | tf_op jit(solution)/shard_map/all_to_all | solution.py:36
  504.7 8.5 %all_to_all.55 = bf16[8,512,16]{1,2,0:T(8,128)(2,1)S(1)} all-to-all(bf16[8,512,16]{1,2,0:T(8,128)(2,1)S(1)} %broadcast_in_dim.19), channel_id=1, replica_groups=mesh['kv_0'=8,'kv_1'=4,'tp'=8] {'tp'}, dimensions={0} | all-to-all | bytes 262144 | tf_op jit(solution)/shard_map/all_to_all | solution.py:22
  513.2 2.2 fusion.36
  515.4 2.1 fusion.37
  517.6 33.1 %reduce-scatter.20.cloned.1.call-done = f32[64,1408]{1,0:T(8,128)} async-done(((f32[512,1408]{1,0:T(8,128)}), f32[64,1408]{1,0:T(8,128)}) %reduce-scatter.20.cloned.1.call-update) | async-done | bytes 360464 | tf_op jit(solution)/shard_map/reduce_scatter | solution.py:42
  550.9 48.0 %reduce-scatter.24.cloned.1.call-done = f32[64,1408]{1,0:T(8,128)} async-done(((f32[512,1408]{1,0:T(8,128)}), f32[64,1408]{1,0:T(8,128)}) %reduce-scatter.24.cloned.1.call-update) | async-done | bytes 360464 | tf_op jit(solution)/shard_map/reduce_scatter | solution.py:42
  599.0 0.7 reduce.11
  599.7 13.1 %all_to_all.56 = bf16[8,2,256]{2,1,0:T(2,128)(2,1)S(1)} all-to-all(bf16[8,2,256]{2,1,0:T(2,128)(2,1)S(1)} %reshape.213), channel_id=1, replica_groups=mesh['kv_0'=8,'kv_1'=4,'tp'=8] {'tp'}, dimensions={0} | all-to-all | bytes 16384 | tf_op jit(solution)/shard_map/all_to_all | solution.py:22
  612.8 12.2 %all-reduce.3 = f32[512]{0:T(512)S(1)} all-reduce(f32[512]{0:T(512)S(1)} %convert_reduce_fusion.3), channel_id=12, replica_groups=mesh['kv_0'=8,'kv_1'=4,'tp'=8] {'kv_0'}, use_global_device_ids=true, to_apply=%region_20.21.clone | all-reduce | flops 512 | bytes 4096
  625.0 8.6 %all-reduce.4 = f32[64]{0:T(128)S(1)} all-reduce(f32[64]{0:T(128)S(1)} %dynamic-slice.7), channel_id=13, replica_groups=mesh['kv_0'=8,'kv_1'=4,'tp'=8] {'kv_1'}, use_global_device_ids=true, to_apply=%region_21.22.clone | all-reduce | flops 64 | bytes 512
  633.8 17.9 %reduce-scatter.26.cloned.1.call-done = f32[16,1408]{1,0:T(8,128)} async-done(((f32[64,1408]{1,0:T(8,128)}), f32[16,1408]{1,0:T(8,128)}) %reduce-scatter.26.cloned.1.call-update) | async-done | bytes 90128 | tf_op jit(solution)/shard_map/reduce_scatter | solution.py:42
  651.7 1.0 multiply_convert_fusion
  652.7 10.4 %all_gather.14 = bf16[64,1408]{1,0:T(8,128)(2,1)} all-gather(bf16[16,1408]{1,0:T(8,128)(2,1)S(1)} %multiply_convert_fusion), channel_id=1, replica_groups=mesh['kv_0'=8,'kv_1'=4,'tp'=8] {'kv_1'}, dimensions={0}, use_global_device_ids=true | all-gather | bytes 225280 | tf_op jit(solution)/shard_map/all_gather | solution.py:49
  663.2 39.8 %all-gather.5.cloned.1.call-done = bf16[512,1408]{1,0:T(8,128)(2,1)} async-done(((bf16[64,1408]{1,0:T(8,128)(2,1)}), bf16[512,1408]{1,0:T(8,128)(2,1)}) %all-gather.5.cloned.1.call-update) | async-done | bytes 1441808 | tf_op jit(solution)/shard_map/all_gather | solution.py:49
  703.0 2.6 convolution_convert_fusion.1
  705.6 9.3 %all-to-all-start.9 = ((bf16[8,512,16]{1,2,0:T(8,128)(2,1)}), bf16[8,512,16]{1,2,0:T(8,128)(2,1)S(1)}, u32[]{:S(2)}, u32[]{:S(2)}) async-start(bf16[8,512,16]{1,2,0:T(8,128)(2,1)} %bitcast.26), calls=%async_computation.17 | async-start | bytes 262144 | tf_op jit(solution)/shard_map/all_to_all | solution.py:36
  714.9 0.6 fusion
  715.5 4.6 all-to-all-done.9
  720.2 0.6 fusion.16
  (117 shorter events, 2.6 us)
Async XLA Ops:
  7.2 11.9 %copy-start = (bf16[128,1408]{1,0:T(8,128)(2,1)S(1)}, bf16[128,1408]{1,0:T(8,128)(2,1)}, u32[]{:S(2)}) copy-start(bf16[128,1408]{1,0:T(8,128)(2,1)} %param.26) | copy-start | bytes 1081348
  7.2 56.3 %reduce-scatter.12.cloned.1.call-start = ((), (), s32[]{:S(2)}) async-start(), calls=%async_computation.19 | async-start | bytes 3244032 | tf_op jit(solution)/shard_map/reduce_scatter | solution.py:42
  19.1 2.2 copy-start.2
  21.2 90.7 %reduce-scatter.16.cloned.1.call-start = ((), (), s32[]{:S(2)}) async-start(), calls=%async_computation.21 | async-start | bytes 3244032 | tf_op jit(solution)/shard_map/reduce_scatter | solution.py:42
  23.4 99.3 %copy-start.23 = (u32[256]{0:T(256)S(1)}, u32[256]{0:T(256)}, u32[]{:S(2)}) copy-start(u32[256]{0:T(256)} %constant.34) | copy-start | bytes 3076
  23.4 99.9 %copy-start.22 = (u32[256]{0:T(256)S(1)}, u32[256]{0:T(256)}, u32[]{:S(2)}) copy-start(u32[256]{0:T(256)} %constant.38) | copy-start | bytes 3076
  23.4 192.9 %copy-start.5 = (bf16[1408,128]{1,0:T(8,128)(2,1)S(1)}, bf16[1408,128]{1,0:T(8,128)(2,1)}, u32[]{:S(2)}) copy-start(bf16[1408,128]{1,0:T(8,128)(2,1)} %param.28) | copy-start | bytes 1081348
  23.5 209.2 %copy-start.11 = (bf16[512,16]{0,1:T(8,128)(2,1)S(1)}, bf16[512,16]{0,1:T(8,128)(2,1)}, u32[]{:S(2)}) copy-start(bf16[512,16]{0,1:T(8,128)(2,1)} %param.22) | copy-start | bytes 49156
  23.5 209.3 %copy-start.17 = (f32[16]{0:T(128)S(1)}, f32[16]{0:T(128)}, u32[]{:S(2)}) copy-start(f32[16]{0:T(128)} %param.29) | copy-start | bytes 196
  23.5 217.8 %copy-start.8 = (bf16[128,512]{1,0:T(8,128)(2,1)S(1)}, bf16[128,512]{1,0:T(8,128)(2,1)}, u32[]{:S(2)}) copy-start(bf16[128,512]{1,0:T(8,128)(2,1)} %param.30) | copy-start | bytes 393220
  23.5 125.6 %reduce-scatter.14.cloned.1.call-start = ((), (), s32[]{:S(2)}) async-start(), calls=%async_computation.20 | async-start | bytes 450560 | tf_op jit(solution)/shard_map/reduce_scatter | solution.py:42
  63.5 101.6 %reduce-scatter.18.cloned.1.call-start = ((), (), s32[]{:S(2)}) async-start(), calls=%async_computation.22 | async-start | bytes 450560 | tf_op jit(solution)/shard_map/reduce_scatter | solution.py:42
  112.0 129.7 %copy-start.9 = (bf16[128,512]{1,0:T(8,128)(2,1)S(1)}, bf16[128,512]{1,0:T(8,128)(2,1)}, u32[]{:S(2)}) copy-start(bf16[128,512]{1,0:T(8,128)(2,1)} %param.31) | copy-start | bytes 393220
  113.9 13.5 %all-to-all-start.1 = ((bf16[8,2,256]{2,1,0:T(2,128)(2,1)}), bf16[8,2,256]{2,1,0:T(2,128)(2,1)S(1)}, u32[]{:S(2)}, u32[]{:S(2)}) async-start(bf16[8,2,256]{2,1,0:T(2,128)(2,1)} %reshape.209), calls=%async_computation.3 | async-start | bytes 16384 | tf_op jit(solution)/shard_map/all_to_all | solution.py:22
  122.7 93.6 %all-gather.3.cloned.1.call-start = ((), (), s32[]{:S(2)}) async-start(), calls=%async_computation.23 | async-start | bytes 1622016 | tf_op jit(solution)/shard_map/all_gather | solution.py:49
  176.6 65.4 %copy-start.12 = (bf16[128,128]{1,0:T(8,128)(2,1)S(1)}, bf16[128,128]{1,0:T(8,128)(2,1)}, u32[]{:S(2)}) copy-start(bf16[128,128]{1,0:T(8,128)(2,1)} %param.32) | copy-start | bytes 98308
  176.6 65.7 %copy-start.13 = (bf16[128,128]{1,0:T(8,128)(2,1)S(1)}, bf16[128,128]{1,0:T(8,128)(2,1)}, u32[]{:S(2)}) copy-start(bf16[128,128]{1,0:T(8,128)(2,1)} %param.33) | copy-start | bytes 98308
  176.6 280.7 %reduce-scatter.28.cloned.1.call-start = ((), (), s32[]{:S(2)}) async-start(), calls=%async_computation.29 | async-start | bytes 2973696 | tf_op jit(solution)/shard_map/reduce_scatter | solution.py:55
  218.4 24.2 %copy-start.15 = (bf16[128,8]{0,1:T(8,128)(2,1)S(1)}, bf16[128,8]{0,1:T(8,128)(2,1)}, u32[]{:S(2)}) copy-start(bf16[128,8]{0,1:T(8,128)(2,1)} %param.34) | copy-start | bytes 6148
  244.9 5.5 copy-start.21
  244.9 6.7 copy-start.14
  244.9 6.7 copy-start.20
  244.9 214.5 %copy-start.7 = (bf16[16,3,1,768]{3,0,2,1:T(8,128)(2,1)S(1)}, bf16[16,3,1,768]{3,0,2,1:T(8,128)(2,1)}, u32[]{:S(2)}) copy-start(bf16[16,3,1,768]{3,0,2,1:T(8,128)(2,1)} %param.24) | copy-start | bytes 221188
  244.9 215.4 %copy-start.19 = (f32[8]{0:T(128)S(1)}, f32[8]{0:T(128)}, u32[]{:S(2)}) copy-start(f32[8]{0:T(128)} %param.36) | copy-start | bytes 100
  246.3 8.7 %all-to-all-start.4 = ((bf16[8,2,256]{2,1,0:T(2,128)(2,1)}), bf16[8,2,256]{2,1,0:T(2,128)(2,1)S(1)}, u32[]{:S(2)}, u32[]{:S(2)}) async-start(bf16[8,2,256]{2,1,0:T(2,128)(2,1)} %reshape.211), calls=%async_computation.8 | async-start | bytes 16384 | tf_op jit(solution)/shard_map/all_to_all | solution.py:22
  250.4 300.4 %reduce-scatter.20.cloned.1.call-start = ((), (), s32[]{:S(2)}) async-start(), calls=%async_computation.24 | async-start | bytes 3244032 | tf_op jit(solution)/shard_map/reduce_scatter | solution.py:42
  463.7 2.0 copy-start.1
  463.7 4.8 copy-start.16
  465.7 22.0 %copy-start.10 = (bf16[512,128]{1,0:T(8,128)(2,1)S(1)}, bf16[512,128]{1,0:T(8,128)(2,1)}, u32[]{:S(2)}) copy-start(bf16[512,128]{1,0:T(8,128)(2,1)} %param.39) | copy-start | bytes 393220
  465.7 38.9 %copy-start.18 = (f32[16]{0:T(128)S(1)}, f32[16]{0:T(128)}, u32[]{:S(2)}) copy-start(f32[16]{0:T(128)} %param.40) | copy-start | bytes 196
  467.4 45.7 %copy-start.3 = (bf16[128,1408]{1,0:T(8,128)(2,1)S(1)}, bf16[128,1408]{1,0:T(8,128)(2,1)}, u32[]{:S(2)}) copy-start(bf16[128,1408]{1,0:T(8,128)(2,1)} %param.41) | copy-start | bytes 1081348
  513.2 2.3 copy-start.4
  515.4 83.5 %reduce-scatter.24.cloned.1.call-start = ((), (), s32[]{:S(2)}) async-start(), calls=%async_computation.26 | async-start | bytes 3244032 | tf_op jit(solution)/shard_map/reduce_scatter | solution.py:42
  517.6 185.4 %copy-start.6 = (bf16[1408,128]{1,0:T(8,128)(2,1)S(1)}, bf16[1408,128]{1,0:T(8,128)(2,1)}, u32[]{:S(2)}) copy-start(bf16[1408,128]{1,0:T(8,128)(2,1)} %param.43) | copy-start | bytes 1081348
  517.6 116.2 %reduce-scatter.22.cloned.1.call-start = ((), (), s32[]{:S(2)}) async-start(), calls=%async_computation.25 | async-start | bytes 450560 | tf_op jit(solution)/shard_map/reduce_scatter | solution.py:42
  550.8 100.9 %reduce-scatter.26.cloned.1.call-start = ((), (), s32[]{:S(2)}) async-start(), calls=%async_computation.27 | async-start | bytes 450560 | tf_op jit(solution)/shard_map/reduce_scatter | solution.py:42
  598.9 104.1 %all-gather.5.cloned.1.call-start = ((), (), s32[]{:S(2)}) async-start(), calls=%async_computation.28 | async-start | bytes 1622016 | tf_op jit(solution)/shard_map/all_gather | solution.py:49
  705.6 14.5 %all-to-all-start.9 = ((bf16[8,512,16]{1,2,0:T(8,128)(2,1)}), bf16[8,512,16]{1,2,0:T(8,128)(2,1)S(1)}, u32[]{:S(2)}, u32[]{:S(2)}) async-start(bf16[8,512,16]{1,2,0:T(8,128)(2,1)} %bitcast.26), calls=%async_computation.17 | async-start | bytes 262144 | tf_op jit(solution)/shard_map/all_to_all | solution.py:36
Sparse Core Ops, SparseCore 0:
  21.4 42.0 reduce-scatter.11
  66.6 45.3 reduce-scatter.15
  114.5 24.6 reduce-scatter.13
  141.6 23.4 reduce-scatter.17
  176.7 39.6 all-gather.2
  245.0 212.3 reduce-scatter.27
  515.5 35.2 reduce-scatter.19
  553.4 45.4 reduce-scatter.23
  601.4 24.5 reduce-scatter.21
  628.4 23.2 reduce-scatter.25
  663.3 39.6 all-gather.4
where the time goes:
time: 728 us; the launch traced here: 727 us
  waiting for transfers between devices  436 us (60%)
  blocking collectives  213 us (29%)
  starting transfers between devices  22.6 us (3%)
  matrix products  16.5 us (2%)
  between operations  16.1 us (2%)
  other arithmetic  12.2 us (2%)
  local copies, waits for them, and re-layouts  10.3 us (1%)
    reduce_scatter x8, waiting for transfers between devices, summed_rows(): array = lax.psum_scatter(array, axis, scatter_dimension=dim, tiled=True)  203 us
    reduce_scatter x1, waiting for transfers between devices, side_by_side(): lax.psum_scatter(both, axis, scatter_dimension=dim, tiled=True)  143 us
    unnamed x5, blocking collectives  102 us
    all_gather x2, waiting for transfers between devices, gathered_by_axis(): result = lax.all_gather(result, axes[number], axis=dim, tiled=True)  79.5 us
    all_to_all x5, blocking collectives, copy_for_each(): return lax.all_to_all(copies, axis, split_axis=0, concat_axis=0, tiled=True)  60.1 us
    all_to_all x2, blocking collectives, sum_at_owner(): lax.all_to_all(tiles, axis, split_axis=0, concat_axis=0, tiled=True)  30.8 us
    all_gather x2, blocking collectives, gathered_by_axis(): result = lax.all_gather(result, axes[number], axis=dim, tiled=True)  20.9 us
  transfers between devices with their start and end apart: 14, of which 12 were waited for; matrix products, arithmetic and copies ran while one was open for 2% of the time, Pallas kernels for 0%

commit v1 on v0

v1 whole, which is shorter than its diff:
```python
import jax
import jax.numpy as jnp
from jax import lax
from jax.experimental import pallas as pl
from jax.experimental.pallas import tpu as pltpu
from jax.sharding import PartitionSpec as P

MESH = pl.DeviceIdType.MESH
F32, BF16 = jnp.float32, jnp.bfloat16

NZ, NX, NY, NC = 8, 4, 4, 2
NKV, NTP = NZ * NX, NY * NC
SEQS, D, FF = 512, 4096, 11264
OWN = D // (NKV * NTP)
FEAT = OWN * NTP
DEPTH = FEAT * NZ
CUT = FF // NTP // NZ
XS = SEQS // NX
ROWS = SEQS // NKV
HEAD, STATE, PER = 64, 128, 8
MIX = 176
WIDE = 256
norm_epsilon = 1e-06
Z_ORDER = (4, 3, 5, 2, 6, 1, 7)


class Wire:
    def __init__(self, sends, recvs):
        self.sends, self.recvs, self.count, self.open = sends, recvs, 0, []
        kv, self.tp = lax.axis_index("kv"), lax.axis_index("tp")
        self.kv = kv
        self.z, self.x = lax.div(kv, NX), lax.rem(kv, NX)
        self.y, self.c = lax.div(self.tp, NC), lax.rem(self.tp, NC)

    def send(self, src, dst, kv, tp):
        number = self.count
        self.count += 1
        copy = pltpu.make_async_remote_copy(
            src_ref=src,
            dst_ref=dst,
            send_sem=self.sends.at[number],
            recv_sem=self.recvs.at[number],
            device_id=(kv, tp),
            device_id_type=MESH,
        )
        copy.start()
        self.open.append(copy)
        return number

    def recv(self, number, dst, kv, tp):
        pltpu.make_async_remote_copy(
            src_ref=dst,
            dst_ref=dst,
            send_sem=self.sends.at[number],
            recv_sem=self.recvs.at[number],
            device_id=(kv, tp),
            device_id_type=MESH,
        ).wait_recv()

    def drain(self):
        for copy in self.open:
            copy.wait_send()
        self.open = []

    def along_z(self, d):
        return lax.rem(self.z + d, NZ)

    def along_x(self, d):
        return lax.rem(self.x + d, NX)

    def along_y(self, d):
        return lax.rem(self.y + d, NY)

    def along_tp(self, d):
        return lax.rem(self.tp + d, NTP)

    def to_z(self, src, dst):
        out = {}
        for d in Z_ORDER:
            peer = self.along_z(d)
            out[d] = self.send(src(peer), dst, peer * NX + self.x, self.tp)
        return out

    def from_z(self, numbers, dst):
        for d in reversed(Z_ORDER):
            peer = self.along_z(NZ - d)
            self.recv(numbers[d], dst(peer), peer * NX + self.x, self.tp)

    def to_x(self, src, dst):
        out = {}
        for d in (2, 1, 3):
            peer = self.along_x(d)
            out[d] = self.send(src(peer), dst, self.z * NX + peer, self.tp)
        return out

    def from_x(self, numbers, dst):
        for d in (1, 3, 2):
            peer = self.along_x(NX - d)
            self.recv(numbers[d], dst(peer), self.z * NX + peer, self.tp)

    def to_y(self, src, dst):
        out = {}
        for d in (2, 1, 3):
            peer = self.along_y(d)
            out[d] = self.send(src(peer), dst, self.kv, peer * NC + self.c)
        return out

    def from_y(self, numbers, dst):
        for d in (1, 3, 2):
            peer = self.along_y(NY - d)
            self.recv(numbers[d], dst(peer), self.kv, peer * NC + self.c)

    def to_tp(self, src, dst):
        out = {}
        for d in range(1, NTP):
            peer = self.along_tp(d)
            out[d] = self.send(src(peer), dst, self.kv, peer)
        return out

    def from_tp(self, numbers, dst):
        for d in range(1, NTP):
            peer = self.along_tp(NTP - d)
            self.recv(numbers[d], dst(peer), self.kv, peer)


def greet(wire, all_kv):
    barrier = pltpu.get_barrier_semaphore()

    def tell(kv, tp):
        pl.semaphore_signal(barrier, inc=1, device_id=(kv, tp), device_id_type=MESH)

    if all_kv:

        @pl.loop(1, NKV)
        def _(d):
            tell(lax.rem(wire.kv + d, NKV), wire.tp)

        count = NKV - 1
    else:
        for d in range(1, NZ):
            tell(wire.along_z(d) * NX + wire.x, wire.tp)
        for d in range(1, NX):
            tell(wire.z * NX + wire.along_x(d), wire.tp)
        count = NZ - 1 + NX - 1
    for d in range(1, NTP):
        tell(wire.kv, wire.along_tp(d))
    count += NTP - 1
    return lambda: pl.semaphore_wait(barrier, count)


def at_rows(start, size, step):
    return pl.ds(pl.multiple_of(start * step, step), size)


def turn_columns(src, dst):
    for j in range(src.shape[1] // 128):
        dst[j * 128 : (j + 1) * 128, :] = src[:, j * 128 : (j + 1) * 128].T


def send_gate_up(wire, gate_t, up_t, both):
    z = wire.z
    lanes = at_rows(z, FEAT, FEAT)

    def cut(ref):
        return lambda peer: ref.at[at_rows(peer, CUT, CUT), :]

    first = wire.to_z(cut(gate_t), both.at[0:CUT, lanes])
    second = wire.to_z(cut(up_t), both.at[CUT : 2 * CUT, lanes])
    own = at_rows(z, CUT, CUT)
    both[0:CUT, lanes] = gate_t[own, :]
    both[CUT : 2 * CUT, lanes] = up_t[own, :]
    return first, second


def wait_gate_up(wire, numbers, both):
    wire.from_z(numbers[0], lambda s: both.at[0:CUT, at_rows(s, FEAT, FEAT)])
    wire.from_z(numbers[1], lambda s: both.at[CUT : 2 * CUT, at_rows(s, FEAT, FEAT)])


def send_down(wire, down, parts):
    numbers = wire.to_z(lambda peer: down.at[at_rows(peer, CUT, CUT), :], parts.at[wire.z])
    parts[wire.z] = down[at_rows(wire.z, CUT, CUT), :]
    return numbers


def wait_down(wire, numbers, parts, turned):
    wire.from_z(numbers, lambda s: parts.at[s])
    for s in range(NZ):
        turned[s] = parts[s].T


def gather_features(wire, values, gain, feats, sq_z, sq_tp, after_first_sends):
    z, tp, y, c = wire.z, wire.tp, wire.y, wire.c
    wide = values.astype(F32)
    feats[z, tp] = (wide * gain[...]).astype(BF16)
    sq_z[z] = jnp.sum(wide * wide, axis=0, keepdims=True)
    n_feats = wire.to_z(lambda peer: feats.at[z, tp], feats.at[z, tp])
    n_sq = wire.to_z(lambda peer: sq_z.at[z], sq_z.at[z])
    after_first_sends()
    wire.from_z(n_feats, lambda s: feats.at[s, tp])
    sibling = y * NC + (1 - c)
    mine = feats.at[:, tp]
    n_y = wire.to_y(lambda peer: mine, mine)
    n_own = wire.send(mine, mine, wire.kv, sibling)
    wire.from_z(n_sq, lambda s: sq_z.at[s])
    sq_tp[tp] = jnp.sum(sq_z[...], axis=0)
    n_sq2 = wire.to_tp(lambda peer: sq_tp.at[tp], sq_tp.at[tp])
    passed = {}
    for d in (1, 3, 2):
        peer = wire.along_y(NY - d)
        block = feats.at[:, peer * NC + c]
        wire.recv(n_y[d], block, wire.kv, peer * NC + c)
        passed[d] = wire.send(block, block, wire.kv, sibling)
    wire.from_tp(n_sq2, lambda s: sq_tp.at[s])
    wire.recv(n_own, feats.at[:, sibling], wire.kv, sibling)
    for d in (1, 3, 2):
        peer = wire.along_y(NY - d)
        wire.recv(passed[d], feats.at[:, peer * NC + 1 - c], wire.kv, sibling)
    return jnp.sum(sq_tp[...], axis=0)


def channel_mixer(wire, values, gain, s, after_first_sends, wait_weights, wait_down_weights, down_t):
    x = wire.x
    squares = gather_features(wire, values, gain, s["feats"], s["sq_z"], s["sq_tp"], after_first_sends)
    s["sq_x"][x] = squares
    n_sq = wire.to_x(lambda peer: s["sq_x"].at[x], s["sq_x"].at[x])
    wait_weights()
    sums = s["sums"]
    sums[...] = jnp.dot(
        s["both"][...], s["feats"][...].reshape(DEPTH, SEQS), preferred_element_type=F32
    ).astype(BF16)
    sums_x = s["sums_x"]
    n_sums = wire.to_x(lambda peer: sums.at[:, at_rows(peer, XS, XS)], sums_x.at[x])
    sums_x[x] = sums[:, at_rows(x, XS, XS)]
    wait_down_weights()
    wire.from_x(n_sq, lambda p: s["sq_x"].at[p])
    factor = lax.rsqrt(jnp.sum(s["sq_x"][...], axis=0) / D + norm_epsilon)
    s["factor"][...] = factor
    factor = s["factor"][:, at_rows(x, XS, XS)]
    wire.from_x(n_sums, lambda p: sums_x.at[p])
    gates = sum(sums_x[p, 0:CUT].astype(F32) for p in range(NX)) * factor
    ups = sum(sums_x[p, CUT : 2 * CUT].astype(F32) for p in range(NX)) * factor
    hidden = s["hidden"]
    here = hidden.at[:, at_rows(x, XS, XS)]
    here[...] = (gates / (1.0 + jnp.exp(-gates)) * ups).astype(BF16)
    n_hidden = wire.to_x(lambda peer: here, here)
    wire.from_x(n_hidden, lambda p: hidden.at[:, at_rows(p, XS, XS)])
    outs = s["outs"]

    @pl.loop(0, NZ)
    def _(k):
        part = jnp.dot(down_t[k], hidden[...], preferred_element_type=F32)
        outs[k] = part.astype(BF16).reshape(NY, NC, OWN, SEQS)

    c, y, z = wire.c, wire.y, wire.z
    sibling = y * NC + (1 - c)
    other = s["other"]
    n_core = wire.send(outs.at[:, :, 1 - c], other, wire.kv, sibling)
    wire.recv(n_core, other, wire.kv, sibling)
    by_y, arrived_y = s["by_y"], s["arrived_y"]

    @pl.loop(0, NZ)
    def _(k):
        total = outs[k, :, c].astype(F32) + other[k].astype(F32)
        by_y[:, k] = total.astype(BF16)

    n_y = wire.to_y(lambda peer: by_y.at[peer], arrived_y.at[y])
    arrived_y[y] = by_y[y]
    wire.from_y(n_y, lambda p: arrived_y.at[p])
    by_z, arrived_z = s["by_z"], s["arrived_z"]
    by_z[...] = sum(arrived_y[p].astype(F32) for p in range(NY)).astype(BF16)
    n_z = wire.to_z(lambda peer: by_z.at[peer], arrived_z.at[z])
    arrived_z[z] = by_z[z]
    wire.from_z(n_z, lambda p: arrived_z.at[p])
    return jnp.sum(arrived_z[...].astype(F32), axis=0)


FF_SCRATCH = dict(
    feats=((NZ, NTP, OWN, SEQS), BF16),
    sq_z=((NZ, 1, SEQS), F32),
    sq_tp=((NTP, 1, SEQS), F32),
    sq_x=((NX, 1, SEQS), F32),
    factor=((1, SEQS), F32),
    gate_t=((NZ * CUT, FEAT), BF16),
    up_t=((NZ * CUT, FEAT), BF16),
    both=((2 * CUT, DEPTH), BF16),
    sums=((2 * CUT, SEQS), BF16),
    sums_x=((NX, 2 * CUT, XS), BF16),
    hidden=((CUT, SEQS), BF16),
    outs=((NZ, NY, NC, OWN, SEQS), BF16),
    other=((NZ, NY, OWN, SEQS), BF16),
    by_y=((NY, NZ, OWN, SEQS), BF16),
    arrived_y=((NY, NZ, OWN, SEQS), BF16),
    by_z=((NZ, OWN, SEQS), BF16),
    arrived_z=((NZ, OWN, SEQS), BF16),
)

A_SCRATCH = dict(
    FF_SCRATCH,
    down_parts=((NZ, CUT, FEAT), BF16),
    down_t=((NZ, FEAT, CUT), BF16),
    next_parts=((NZ, CUT, FEAT), BF16),
    mix_t=((NZ, MIX, FEAT), BF16),
    mix_in=((MIX, DEPTH), BF16),
    mix_feats=((NZ, NTP, OWN, SEQS), BF16),
    mix_sq_z=((NZ, 1, SEQS), F32),
    mix_sq_tp=((NTP, 1, SEQS), F32),
    turned=((WIDE, SEQS), F32),
    rows=((NKV, ROWS, WIDE), BF16),
    rows_in=((NKV, ROWS, WIDE), BF16),
)

B_SCRATCH = dict(
    FF_SCRATCH,
    mixed_all=((NZ, NX, ROWS, PER * HEAD), BF16),
    out_t=((NTP, OWN, SEQS), BF16),
    out_in=((NTP, OWN, SEQS), BF16),
)


def before_state(*refs):
    (stream, gain, mix_gain, gate, up, down, gate_in, value_in, write_in, read_in, step_in, next_down) = refs[:12]
    after_first, projected, next_down_t = refs[12:15]
    s = dict(zip(A_SCRATCH, refs[15:]))
    wire = Wire(*refs[15 + len(A_SCRATCH) : 17 + len(A_SCRATCH)])
    row_sends, row_recvs = refs[17 + len(A_SCRATCH) :]
    z, x, kv, tp = wire.z, wire.x, wire.kv, wire.tp
    wait_greeting = greet(wire, True)
    turn_columns(gate, s["gate_t"])
    turn_columns(up, s["up_t"])
    wait_greeting()

    def turn_mixer():
        for j in range(PER * HEAD // 128):
            for ref, at in ((gate_in, 0), (value_in, HEAD)):
                tile = ref[:, j * 128 : (j + 1) * 128].T
                s["mix_t"][2 * j, at : at + HEAD] = tile[:HEAD]
                s["mix_t"][2 * j + 1, at : at + HEAD] = tile[HEAD:]
        for ref, base in ((write_in, 0), (read_in, 4)):
            tile = ref[...].T
            for j in range(4):
                s["mix_t"][base + j, 2 * HEAD : 2 * HEAD + 32] = tile[32 * j : 32 * (j + 1)]
        for j in range(NZ):
            s["mix_t"][j, 2 * HEAD + 32 : MIX] = step_in[...]

    numbers = {}

    def weights_out():
        numbers["both"] = send_gate_up(wire, s["gate_t"], s["up_t"], s["both"])
        numbers["down"] = send_down(wire, down, s["down_parts"])
        turn_mixer()
        lanes = at_rows(z, FEAT, FEAT)
        numbers["mix"] = wire.to_z(lambda peer: s["mix_t"].at[peer], s["mix_in"].at[:, lanes])
        s["mix_in"][:, lanes] = s["mix_t"][z]

    branch = channel_mixer(
        wire,
        stream[...],
        gain,
        s,
        weights_out,
        lambda: wait_gate_up(wire, numbers["both"], s["both"]),
        lambda: wait_down(wire, numbers["down"], s["down_parts"], s["down_t"]),
        s["down_t"],
    )
    after = (stream[...].astype(F32) + 0.5 * branch).astype(BF16)
    after_first[...] = after

    def next_weights():
        numbers["next"] = send_down(wire, next_down, s["next_parts"])

    squares = gather_features(wire, after, mix_gain, s["mix_feats"], s["mix_sq_z"], s["mix_sq_tp"], next_weights)
    wire.from_z(numbers["mix"], lambda p: s["mix_in"].at[:, at_rows(p, FEAT, FEAT)])
    part = jnp.dot(s["mix_in"][...], s["mix_feats"][...].reshape(DEPTH, SEQS), preferred_element_type=F32)
    turned = s["turned"]
    turned[2 * HEAD :, :] = jnp.zeros((WIDE - 2 * HEAD, SEQS), F32)
    turned[: 2 * HEAD, :] = part[: 2 * HEAD]
    quarter = lax.rem(z, 4)
    turned[pl.ds(pl.multiple_of(128 + 32 * quarter, 32), 32), :] = part[2 * HEAD : 2 * HEAD + 32]
    beside = pl.multiple_of(128 + 32 * lax.rem(z + 1, 4), 32)
    turned[pl.ds(beside, 8), :] = part[2 * HEAD + 32 : 2 * HEAD + 40]
    turned[pl.ds(pl.multiple_of(beside + 8, 8), 8), :] = jnp.broadcast_to(squares, (8, SEQS))
    rows, rows_in = s["rows"], s["rows_in"]
    rows[...] = turned[...].T.astype(BF16).reshape(NKV, ROWS, WIDE)

    def row_copy(d, peer, slot):
        return pltpu.make_async_remote_copy(
            src_ref=rows.at[peer],
            dst_ref=rows_in.at[slot],
            send_sem=row_sends.at[d],
            recv_sem=row_recvs.at[d],
            device_id=(peer, tp),
            device_id_type=MESH,
        )

    @pl.loop(1, NKV)
    def _(d):
        row_copy(d, lax.rem(kv + d, NKV), kv).start()

    rows_in[kv] = rows[kv]
    wire.from_z(numbers["next"], lambda p: s["next_parts"].at[p])
    for k in range(NZ):
        next_down_t[k] = s["next_parts"][k].T

    @pl.loop(1, NKV)
    def _(d):
        peer = lax.rem(kv + NKV - d, NKV)
        row_copy(d, peer, peer).wait_recv()

    for k in range(NZ):
        projected[k] = sum(rows_in[k * NX + p].astype(F32) for p in range(NX))

    wire.drain()

    @pl.loop(1, NKV)
    def _(d):
        row_copy(d, lax.rem(kv + d, NKV), kv).wait_send()


def after_state(*refs):
    (after_first, mixed, out_weight, gain, gate, up, down_t) = refs[:7]
    result = refs[7]
    s = dict(zip(B_SCRATCH, refs[8:]))
    wire = Wire(*refs[8 + len(B_SCRATCH) :])
    z, x, kv, tp = wire.z, wire.x, wire.kv, wire.tp
    wait_greeting = greet(wire, False)
    mixed_all = s["mixed_all"]
    mixed_all[z, x] = mixed[...]
    wait_greeting()
    n_z = wire.to_z(lambda peer: mixed_all.at[z, x], mixed_all.at[z, x])
    turn_columns(gate, s["gate_t"])
    turn_columns(up, s["up_t"])
    n_both = send_gate_up(wire, s["gate_t"], s["up_t"], s["both"])
    wire.from_z(n_z, lambda p: mixed_all.at[p, x])
    column = mixed_all.at[:, x]
    n_x = wire.to_x(lambda peer: column, column)
    wire.from_x(n_x, lambda p: mixed_all.at[:, p])
    part = jnp.dot(mixed_all[...].reshape(SEQS, PER * HEAD), out_weight[...], preferred_element_type=F32)
    out_t, out_in = s["out_t"], s["out_in"]
    out_t[...] = part.T.astype(BF16).reshape(NTP, OWN, SEQS)
    n_tp = wire.to_tp(lambda peer: out_t.at[peer], out_in.at[tp])
    out_in[tp] = out_t[tp]
    wire.from_tp(n_tp, lambda p: out_in.at[p])
    after = (after_first[...].astype(F32) + jnp.sum(out_in[...].astype(F32), axis=0)).astype(BF16)
    branch = channel_mixer(
        wire,
        after,
        gain,
        s,
        lambda: None,
        lambda: wait_gate_up(wire, n_both, s["both"]),
        lambda: None,
        down_t,
    )
    result[...] = (after.astype(F32) + 0.5 * branch).astype(BF16)
    wire.drain()


def call(body, name, number, outs, scratch, copies, extra, *args):
    memory = [pltpu.VMEM(shape, dtype) for shape, dtype in scratch.values()]
    memory += [pltpu.SemaphoreType.DMA((copies,))] * 2
    memory += extra
    whole = pl.BlockSpec(memory_space=pltpu.VMEM)
    return pl.pallas_call(
        body,
        name=name,
        out_shape=outs,
        in_specs=[whole] * len(args),
        out_specs=jax.tree.map(lambda _: whole, outs),
        scratch_shapes=memory,
        compiler_params=pltpu.CompilerParams(
            collective_id=number, has_side_effects=True, vmem_limit_bytes=48 * 1024 * 1024
        ),
    )(*args)


def state_update(
    projected, ssm_state, conv_state, conv_weight, step_bias, log_decay_rate, group_gain
):
    total = projected[3, :, 2 * HEAD + 8]
    factor = lax.rsqrt(total / D + norm_epsilon)
    scaled = (projected * factor[None, :, None]).astype(BF16)
    gate = scaled[:, :, :HEAD].transpose(1, 0, 2)
    values = scaled[:, :, HEAD : 2 * HEAD].transpose(1, 0, 2).reshape(ROWS, PER * HEAD)
    tile = scaled[:, :, 2 * HEAD :]
    shared = [tile[k, :, 32 * (k % 4) : 32 * (k % 4) + 32] for k in range(NZ)]
    steps = tile[3, :, :PER]
    fresh = jnp.concatenate([values, *shared], axis=1)
    window = jnp.concatenate([conv_state[:, :, 0], fresh[:, None]], axis=1)
    activated = jax.nn.silu(jnp.sum(window.astype(F32) * conv_weight[None, :, 0], axis=1))
    inputs = activated[:, : PER * HEAD].reshape(ROWS, PER, HEAD)
    write_vec = activated[:, PER * HEAD : PER * HEAD + STATE]
    read_vec = activated[:, PER * HEAD + STATE :]
    step_size = jax.nn.softplus(steps.astype(F32) + step_bias[None])
    decay = jnp.exp(-step_size * jnp.exp(log_decay_rate)[None])
    updated = (
        ssm_state * decay[:, :, None, None]
        + (step_size[:, :, None] * inputs)[..., None] * write_vec[:, None, None, :]
    )
    readout = jnp.einsum("bhpn,bn->bhp", updated, read_vec)
    gated = (readout * jax.nn.silu(gate.astype(F32))).reshape(ROWS, PER * HEAD)
    normed = gated * lax.rsqrt(jnp.mean(gated * gated, axis=1, keepdims=True) + norm_epsilon)
    mixed = (normed * group_gain[None]).astype(BF16)
    return mixed, updated, window[:, 1:, None]


def on_device(
    stream,
    ssm_state,
    conv_state,
    first_gain,
    first_gate,
    first_up,
    first_down,
    mix_gain,
    gate_in,
    value_in,
    write_in,
    read_in,
    step_in,
    conv_weight,
    step_bias,
    log_decay_rate,
    group_gain,
    out_weight,
    last_norm_gain,
    second_gate,
    second_up,
    second_down,
):
    step_t = jnp.pad(step_in.T, ((0, MIX - 2 * HEAD - 32 - PER), (0, 0)))
    after_first, projected, next_down_t = call(
        before_state,
        "before_state",
        0,
        (
            jax.ShapeDtypeStruct((OWN, SEQS), BF16),
            jax.ShapeDtypeStruct((NZ, ROWS, WIDE), F32),
            jax.ShapeDtypeStruct((NZ, FEAT, CUT), BF16),
        ),
        A_SCRATCH,
        140,
        [pltpu.SemaphoreType.DMA((NKV,))] * 2,
        stream.T,
        first_gain[:, None],
        mix_gain[:, None],
        first_gate,
        first_up,
        first_down,
        gate_in,
        value_in,
        write_in,
        read_in,
        step_t,
        second_down,
    )
    mixed, ssm_next, conv_next = state_update(
        projected, ssm_state, conv_state, conv_weight, step_bias, log_decay_rate, group_gain
    )
    result = call(
        after_state,
        "after_state",
        1,
        jax.ShapeDtypeStruct((OWN, SEQS), BF16),
        B_SCRATCH,
        100,
        [],
        after_first,
        mixed,
        out_weight,
        last_norm_gain[:, None],
        second_gate,
        second_up,
        next_down_t,
    )
    return (result.T, ssm_next, conv_next)


def solution(mesh):
    placed = (
        P(None, ("kv", "tp")),
        P("kv", "tp", None, None),
        P("kv", None, "tp", None),
        P(("kv", "tp")),
        P("kv", "tp"),
        P("kv", "tp"),
        P("tp", "kv"),
        P(("kv", "tp")),
        P("kv", "tp"),
        P("kv", "tp"),
        P("kv", "tp"),
        P("kv", "tp"),
        P("kv", "tp"),
        P(None, "tp", None),
        P("tp"),
        P("tp"),
        P("tp"),
        P("tp", "kv"),
        P(("kv", "tp")),
        P("kv", "tp"),
        P("kv", "tp"),
        P("tp", "kv"),
    )
    return jax.shard_map(
        on_device,
        mesh=mesh,
        in_specs=placed,
        out_specs=(P(None, ("kv", "tp")), P("kv", "tp", None, None), P("kv", None, "tp", None)),
        check_vma=False,
    )
```

time: 728 us -> 180 us (0.25)
  waiting for transfers between devices: 436 us -> 0 us
  blocking collectives: 213 us -> 0 us
  Pallas kernels: 0 us -> 156 us
  starting transfers between devices: 22.6 us -> 0 us
  between operations: 16.1 us -> 0.81 us
  matrix products: 16.5 us -> 1.71 us
    reduce_scatter x9 -> x0, waiting for transfers between devices: 346 us -> none  [the longest x8 203 us: summed_rows(): array = lax.psum_scatter(array, axis, scatter_dimension=dim, tiled=True)]
    pallas_call x0 -> x2, Pallas kernels: none -> 156 us  [call(): pl.pallas_call(body, name=name, out_shape=outs, in_specs=[whole] * len(ar...]
    unnamed x5 -> x0, blocking collectives: 102 us -> none
    all_to_all x7 -> x0, blocking collectives: 90.9 us -> none  [the longest x5 60.1 us: copy_for_each(): return lax.all_to_all(copies, axis, split_axis=0, concat_axis=0, tiled=True)]
    all_gather x2 -> x0, waiting for transfers between devices: 79.5 us -> none  [gathered_by_axis(): result = lax.all_gather(result, axes[number], axis=dim, tiled=True)]
    all_to_all x3 -> x0, starting transfers between devices: 22.2 us -> none  [the longest x2 13 us: copy_for_each(): return lax.all_to_all(copies, axis, split_axis=0, concat_axis=0, tiled=True)]
    all_gather x2 -> x0, blocking collectives: 20.9 us -> none  [gathered_by_axis(): result = lax.all_gather(result, axes[number], axis=dim, tiled=True)]
    dot_general x13 -> x1, matrix products: 16.5 us -> 1.71 us  [state_update(): readout = jnp.einsum('bhpn,bn->bhp', updated, read_vec)]
  transfers between devices with their start and end apart: 14 -> 0, of which waited for: 12 -> 0; matrix products, arithmetic and copies ran while one was open for 2% -> 0% of each run, Pallas kernels for 0% -> 0%
where the time goes in v1:
time: 180 us; the launch traced here: 179 us
  Pallas kernels  156 us (87%)
  local copies, waits for them, and re-layouts  14.9 us (8%)
  other arithmetic  5.96 us (3%)
    pallas_call x2, Pallas kernels, call(): pl.pallas_call(body, name=name, out_shape=outs, in_specs=[whole] * len(ar...  156 us
    unnamed x34, local copies, waits for them, and re-layouts  11.3 us

profile of v1, /device:TPU:1, one launch (start us, length us, event | category | flops | bytes accessed | tf_op | source)
XLA Modules:
  0.0 179.3 jit_solution(3886922878227692891)
XLA Ops:
  0.6 0.7 copy.40.refs_1_
  1.4 0.7 copy.41.refs_2_
  2.1 0.7 pad.4.refs_10_
  2.8 0.0 copy-start
  2.8 1.0 copy-done
  3.8 0.0 copy-start.1
  3.8 1.0 copy-done.1
  4.7 0.0 copy-start.2
  4.8 1.0 copy-done.2
  5.7 0.0 copy-start.3
  5.7 1.0 copy-done.3
  6.7 0.0 copy-start.6
  6.7 0.9 copy-done.6
  7.6 0.0 copy-start.7
  7.6 0.9 copy-done.7
  8.5 0.0 copy-start.9
  8.5 0.8 copy-done.9
  9.3 0.0 copy-start.10
  9.3 0.8 copy-done.10
  10.0 0.0 copy-start.11
  10.0 0.7 copy-done.11
  10.8 89.1 %before_state.1 = (bf16[16,512]{1,0:T(8,128)(2,1)S(1)}, f32[8,16,256]{2,1,0:T(8,128)S(1)}, bf16[8,128,176]{2,1,0:T(8,128)(2,1)S(1)}) custom-call(bf16[16,512]{1,0:T(8,128)(2,1)S(1)} %bitcast.59, f32[16,1]{1,0:T(8,128)S(1)} %copy.40.refs_1_, f32[16,1]{1,0:T(8,128)S(1)} %copy.41.refs_2_, bf16[128,1408]{1,0:T(8,128)(2,1)S(1)} %copy-done, ...), custom_call_target="tpu_custom_call" | custom-call | tf_op jit(solution)/shard_map/before_state/pallas_call | solution.py:464
  99.9 0.2 rsqrt_reduce_fusion
  100.1 0.1 multiply_convert_fusion
  100.2 0.1 slice_bitcast_fusion.1
  100.3 0.1 slice_bitcast_fusion
  100.4 0.1 reshape.95
  100.5 0.1 concatenate.6
  100.6 0.7 copy.54
  101.3 0.9 multiply_reduce_fusion
  102.2 0.1 reshape.96
  102.3 0.1 copy.42
  102.4 0.7 exp.31
  103.1 0.7 multiply_exponential_fusion
  103.8 0.1 copy.44
  103.9 0.1 broadcast_multiply_fusion
  104.0 0.1 copy.43
  104.1 3.0 %multiply_add_fusion = f32[16,8,64,128]{3,2,1,0:T(8,128)S(1)} fusion(f32[16,8,64,128]{3,2,1,0:T(8,128)} %param.23, f32[16,128]{1,0:T(8,128)S(1)} %get-tuple-element.22, f32[16,8,64]{2,1,0:T(8,128)S(1)} %broadcast_multiply_fusion, f32[16,8]{1,0:T(8,128)S(1)} %copy.43), kind=kLoop, calls=%fused_computation | loop fusion | flops 3145728 | bytes 8430080 | tf_op jit(solution)/shard_map/add | solution.py:497
  107.1 0.0 copy-start.12
  107.1 0.0 copy-start.14
  107.1 0.0 copy-start.15
  107.1 0.0 copy-start.4
  107.2 0.0 copy-start.5
  107.2 0.0 copy-start.8
  107.2 0.0 copy-start.13
  107.2 1.9 %copy-done.12 = f32[16,8,64,128]{3,2,1,0:T(8,128)} copy-done((f32[16,8,64,128]{3,2,1,0:T(8,128)}, f32[16,8,64,128]{3,2,1,0:T(8,128)S(1)}, u32[]{:S(2)}) %copy-start.12) | copy-done | bytes 4194328
  109.1 1.7 fusion.8
  110.8 0.2 multiply_reduce_fusion.1
  111.0 0.1 reshape.97
  111.1 0.0 copy-done.14
  111.1 0.1 multiply_convert_fusion.1.refs_1_
  111.2 0.0 copy-done.15
  111.2 0.1 copy.47.refs_3_
  111.3 0.0 copy-done.4
  111.3 0.0 copy-done.5
  111.3 0.0 copy-done.8
  111.3 66.7 %after_state.1 = bf16[16,512]{1,0:T(8,128)(2,1)S(1)} custom-call(bf16[16,512]{1,0:T(8,128)(2,1)S(1)} %get-tuple-element.6.refs_0_, bf16[16,512]{1,0:T(8,128)(2,1)S(1)} %multiply_convert_fusion.1.refs_1_, bf16[512,128]{1,0:T(8,128)(2,1)S(1)} %copy-done.8, f32[16,1]{1,0:T(8,128)S(1)} %copy.47.refs_3_, bf16[128,1408]{1,0:T(8,128)(2,1)S(1)} %copy-done.4, ...), custom_call_target="tpu_custom_call" | custom-call | tf_op jit(solution)/shard_map/after_state/pallas_call | solution.py:464
  178.0 0.0 copy-done.13
  178.1 0.6 fusion.1
  178.7 0.6 copy.56
  (7 shorter events, 0.1 us)
Async XLA Ops:
  2.8 1.0 copy-start
  3.8 1.0 copy-start.1
  4.7 1.0 copy-start.2
  5.7 1.0 copy-start.3
  6.7 0.9 copy-start.6
  7.6 0.9 copy-start.7
  8.5 0.8 copy-start.9
  9.3 0.8 copy-start.10
  10.0 0.7 copy-start.11
  107.1 2.0 %copy-start.12 = (f32[16,8,64,128]{3,2,1,0:T(8,128)}, f32[16,8,64,128]{3,2,1,0:T(8,128)S(1)}, u32[]{:S(2)}) copy-start(f32[16,8,64,128]{3,2,1,0:T(8,128)S(1)} %multiply_add_fusion) | copy-start | bytes 12582916
  107.1 4.0 %copy-start.14 = (f32[512]{0:T(512)S(1)}, f32[512]{0:T(512)}, u32[]{:S(2)}) copy-start(f32[512]{0:T(512)} %param.38) | copy-start | bytes 6148
  107.1 4.1 %copy-start.15 = (f32[16]{0:T(128)S(1)}, f32[16]{0:T(128)}, u32[]{:S(2)}) copy-start(f32[16]{0:T(128)} %param.40) | copy-start | bytes 196
  107.1 4.1 %copy-start.4 = (bf16[128,1408]{1,0:T(8,128)(2,1)S(1)}, bf16[128,1408]{1,0:T(8,128)(2,1)}, u32[]{:S(2)}) copy-start(bf16[128,1408]{1,0:T(8,128)(2,1)} %refs_4_.3) | copy-start | bytes 1081348
  107.2 4.1 %copy-start.5 = (bf16[128,1408]{1,0:T(8,128)(2,1)S(1)}, bf16[128,1408]{1,0:T(8,128)(2,1)}, u32[]{:S(2)}) copy-start(bf16[128,1408]{1,0:T(8,128)(2,1)} %refs_5_.3) | copy-start | bytes 1081348
  107.2 4.1 %copy-start.8 = (bf16[512,128]{1,0:T(8,128)(2,1)S(1)}, bf16[512,128]{1,0:T(8,128)(2,1)}, u32[]{:S(2)}) copy-start(bf16[512,128]{1,0:T(8,128)(2,1)} %refs_2_.1) | copy-start | bytes 393220
  107.2 70.9 %copy-start.13 = (bf16[16,3,1,768]{3,0,2,1:T(8,128)(2,1)S(1)}, bf16[16,3,1,768]{3,0,2,1:T(8,128)(2,1)}, u32[]{:S(2)}) copy-start(bf16[16,3,1,768]{3,0,2,1:T(8,128)(2,1)} %param.24) | copy-start | bytes 221188

commit v2 on v1

v2 whole, which is shorter than its diff:
```python
import jax
import jax.numpy as jnp
from jax import lax
from jax.experimental import pallas as pl
from jax.experimental.pallas import tpu as pltpu
from jax.sharding import PartitionSpec as P

MESH = pl.DeviceIdType.MESH
F32, BF16 = jnp.float32, jnp.bfloat16

NZ, NX, NY, NC = 8, 4, 4, 2
NKV, NTP = NZ * NX, NY * NC
SEQS, D, FF = 512, 4096, 11264
OWN = D // (NKV * NTP)
FEAT = OWN * NTP
DEPTH = FEAT * NZ
CUT = FF // NTP // NZ
XS = SEQS // NX
ROWS = SEQS // NKV
HEAD, STATE, PER = 64, 128, 8
MIX = 176
WIDE = 256
norm_epsilon = 1e-06
Z_ORDER = (4, 3, 5, 2, 6, 1, 7)
Z_NEAR = (1, 7, 2, 6, 3, 5, 4)


class Wire:
    def __init__(self, sends, recvs):
        self.sends, self.recvs, self.count, self.open = sends, recvs, 0, []
        kv, self.tp = lax.axis_index("kv"), lax.axis_index("tp")
        self.kv = kv
        self.z, self.x = lax.div(kv, NX), lax.rem(kv, NX)
        self.y, self.c = lax.div(self.tp, NC), lax.rem(self.tp, NC)

    def send(self, src, dst, kv, tp):
        number = self.count
        self.count += 1
        copy = pltpu.make_async_remote_copy(
            src_ref=src,
            dst_ref=dst,
            send_sem=self.sends.at[number],
            recv_sem=self.recvs.at[number],
            device_id=(kv, tp),
            device_id_type=MESH,
        )
        copy.start()
        self.open.append(copy)
        return number

    def recv(self, number, dst, kv, tp):
        pltpu.make_async_remote_copy(
            src_ref=dst,
            dst_ref=dst,
            send_sem=self.sends.at[number],
            recv_sem=self.recvs.at[number],
            device_id=(kv, tp),
            device_id_type=MESH,
        ).wait_recv()

    def drain(self):
        for copy in self.open:
            copy.wait_send()
        self.open = []

    def along_z(self, d):
        return lax.rem(self.z + d, NZ)

    def along_x(self, d):
        return lax.rem(self.x + d, NX)

    def along_y(self, d):
        return lax.rem(self.y + d, NY)

    def along_tp(self, d):
        return lax.rem(self.tp + d, NTP)

    def to_z(self, src, dst):
        out = {}
        for d in Z_ORDER:
            peer = self.along_z(d)
            out[d] = self.send(src(peer), dst, peer * NX + self.x, self.tp)
        return out

    def from_z(self, numbers, dst):
        for d in reversed(Z_ORDER):
            peer = self.along_z(NZ - d)
            self.recv(numbers[d], dst(peer), peer * NX + self.x, self.tp)

    def to_x(self, src, dst):
        out = {}
        for d in (2, 1, 3):
            peer = self.along_x(d)
            out[d] = self.send(src(peer), dst, self.z * NX + peer, self.tp)
        return out

    def from_x(self, numbers, dst):
        for d in (1, 3, 2):
            peer = self.along_x(NX - d)
            self.recv(numbers[d], dst(peer), self.z * NX + peer, self.tp)

    def to_y(self, src, dst):
        out = {}
        for d in (2, 1, 3):
            peer = self.along_y(d)
            out[d] = self.send(src(peer), dst, self.kv, peer * NC + self.c)
        return out

    def from_y(self, numbers, dst):
        for d in (1, 3, 2):
            peer = self.along_y(NY - d)
            self.recv(numbers[d], dst(peer), self.kv, peer * NC + self.c)

    def to_tp(self, src, dst):
        out = {}
        for d in range(1, NTP):
            peer = self.along_tp(d)
            out[d] = self.send(src(peer), dst, self.kv, peer)
        return out

    def from_tp(self, numbers, dst):
        for d in range(1, NTP):
            peer = self.along_tp(NTP - d)
            self.recv(numbers[d], dst(peer), self.kv, peer)


def greet(wire):
    barrier = pltpu.get_barrier_semaphore()

    def tell(kv, tp):
        pl.semaphore_signal(barrier, inc=1, device_id=(kv, tp), device_id_type=MESH)

    for d in range(1, NZ):
        tell(wire.along_z(d) * NX + wire.x, wire.tp)
    for d in range(1, NX):
        tell(wire.z * NX + wire.along_x(d), wire.tp)
    for d in range(1, NTP):
        tell(wire.kv, wire.along_tp(d))
    return lambda: pl.semaphore_wait(barrier, NZ - 1 + NX - 1 + NTP - 1)


def at_rows(start, size, step):
    return pl.ds(pl.multiple_of(start * step, step), size)


def turn_columns(src, dst):
    for j in range(src.shape[1] // 128):
        dst[j * 128 : (j + 1) * 128, :] = src[:, j * 128 : (j + 1) * 128].T


def send_turned(wire, turned, both, at):
    z = wire.z
    lanes = at_rows(z, FEAT, FEAT)
    place = both.at[at : at + CUT, lanes]
    numbers = wire.to_z(lambda peer: turned.at[at_rows(peer, CUT, CUT), :], place)
    both[at : at + CUT, lanes] = turned[at_rows(z, CUT, CUT), :]
    return numbers


def wait_turned(wire, numbers, both, at):
    wire.from_z(numbers, lambda s: both.at[at : at + CUT, at_rows(s, FEAT, FEAT)])


def send_down(wire, down, parts):
    numbers = wire.to_z(lambda peer: down.at[at_rows(peer, CUT, CUT), :], parts.at[wire.z])
    parts[wire.z] = down[at_rows(wire.z, CUT, CUT), :]
    return numbers


def wait_down(wire, numbers, parts, turned):
    wire.from_z(numbers, lambda s: parts.at[s])
    for s in range(NZ):
        turned[s] = parts[s].T


def as_column(row):
    square = jnp.broadcast_to(row, (OWN, OWN))
    same = lax.broadcasted_iota(jnp.int32, (OWN, OWN), 0) == lax.broadcasted_iota(jnp.int32, (OWN, OWN), 1)
    return jnp.sum(jnp.where(same, square, 0.0), axis=1, keepdims=True)


def gather_features(wire, values, gain, feats, sq_z, sq_tp, after_first_sends):
    z, tp, y, c = wire.z, wire.tp, wire.y, wire.c
    sibling = y * NC + (1 - c)
    wide = values.astype(F32)
    feats[z, tp] = (wide * as_column(gain[...])).astype(BF16)
    own = feats.at[z, tp]
    n_feats = {}
    for d in Z_NEAR:
        n_feats[d] = wire.send(own, own, wire.along_z(d) * NX + wire.x, tp)
    n_y, n_core, n_passed = {}, {}, {}

    def hand_on(d, peer):
        block = feats.at[peer, tp]
        n_y[d] = wire.to_y(lambda p: block, block)
        n_core[d] = wire.send(block, block, wire.kv, sibling)

    def pass_on(d, peer):
        for e in (1, 3, 2):
            source = wire.along_y(NY - e) * NC + c
            block = feats.at[peer, source]
            wire.recv(n_y[d][e], block, wire.kv, source)
            n_passed[d, e] = wire.send(block, block, wire.kv, sibling)

    hand_on(0, z)
    sq_z[z] = jnp.sum(wide * wide, axis=0, keepdims=True)
    n_sq = wire.to_z(lambda peer: sq_z.at[z], sq_z.at[z])
    after_first_sends()
    steps = [(0, z)] + [(d, wire.along_z(NZ - d)) for d in Z_NEAR]
    for d, peer in steps[1:]:
        wire.recv(n_feats[d], feats.at[peer, tp], peer * NX + wire.x, tp)
        hand_on(d, peer)
    wire.from_z(n_sq, lambda s: sq_z.at[s])
    sq_tp[tp] = jnp.sum(sq_z[...], axis=0)
    n_sq2 = wire.to_tp(lambda peer: sq_tp.at[tp], sq_tp.at[tp])
    for d, peer in steps:
        pass_on(d, peer)
    wire.from_tp(n_sq2, lambda s: sq_tp.at[s])
    for d, peer in steps:
        wire.recv(n_core[d], feats.at[peer, sibling], wire.kv, sibling)
        for e in (1, 3, 2):
            source = wire.along_y(NY - e) * NC + 1 - c
            wire.recv(n_passed[d, e], feats.at[peer, source], wire.kv, sibling)
    return jnp.sum(sq_tp[...], axis=0)


def channel_mixer(wire, values, gain, s, after_first_sends, wait_weights, wait_down_weights, down_t):
    x = wire.x
    squares = gather_features(wire, values, gain, s["feats"], s["sq_z"], s["sq_tp"], after_first_sends)
    s["sq_x"][x] = squares
    n_sq = wire.to_x(lambda peer: s["sq_x"].at[x], s["sq_x"].at[x])
    wait_weights()
    sums = s["sums"]
    sums[...] = jnp.dot(
        s["both"][...], s["feats"][...].reshape(DEPTH, SEQS), preferred_element_type=F32
    ).astype(BF16)
    sums_x = s["sums_x"]
    n_sums = wire.to_x(lambda peer: sums.at[:, at_rows(peer, XS, XS)], sums_x.at[x])
    sums_x[x] = sums[:, at_rows(x, XS, XS)]
    wire.from_x(n_sq, lambda p: s["sq_x"].at[p])
    s["factor"][...] = lax.rsqrt(jnp.sum(s["sq_x"][...], axis=0) / D + norm_epsilon)
    factor = s["factor"][:, at_rows(x, XS, XS)]
    wire.from_x(n_sums, lambda p: sums_x.at[p])
    gates = sum(sums_x[p, 0:CUT].astype(F32) for p in range(NX)) * factor
    ups = sum(sums_x[p, CUT : 2 * CUT].astype(F32) for p in range(NX)) * factor
    hidden = s["hidden"]
    here = hidden.at[:, at_rows(x, XS, XS)]
    here[...] = (gates / (1.0 + jnp.exp(-gates)) * ups).astype(BF16)
    n_hidden = wire.to_x(lambda peer: here, here)
    wait_down_weights()
    wire.from_x(n_hidden, lambda p: hidden.at[:, at_rows(p, XS, XS)])

    c, y, z = wire.c, wire.y, wire.z
    sibling = y * NC + (1 - c)
    outs, other = s["outs"], s["other"]
    by_y, arrived_y = s["by_y"], s["arrived_y"]
    by_z, arrived_z = s["by_z"], s["arrived_z"]
    order = [(d, wire.along_z(d)) for d in Z_ORDER + (0,)]
    n_core, n_y, n_z = {}, {}, {}
    for d, k in order:
        part = jnp.dot(down_t[k], hidden[...], preferred_element_type=F32)
        outs[k] = part.astype(BF16).reshape(NY, NC, OWN, SEQS)
        n_core[d] = wire.send(outs.at[k, :, 1 - c], other.at[k], wire.kv, sibling)
    for d, k in order:
        wire.recv(n_core[d], other.at[k], wire.kv, sibling)
        by_y[:, k] = (outs[k, :, c].astype(F32) + other[k].astype(F32)).astype(BF16)
        n_y[d] = wire.to_y(lambda peer, k=k: by_y.at[peer, k], arrived_y.at[y, k])
        arrived_y[y, k] = by_y[y, k]
    for d, k in order:
        wire.from_y(n_y[d], lambda p, k=k: arrived_y.at[p, k])
        by_z[k] = sum(arrived_y[p, k].astype(F32) for p in range(NY)).astype(BF16)
        if d:
            n_z[d] = wire.send(by_z.at[k], arrived_z.at[z], k * NX + wire.x, wire.tp)
    arrived_z[z] = by_z[z]
    wire.from_z(n_z, lambda p: arrived_z.at[p])
    return jnp.sum(arrived_z[...].astype(F32), axis=0)


def ff_scratch(name):
    return {
        name + key: value
        for key, value in dict(
            feats=((NZ, NTP, OWN, SEQS), BF16),
            sq_z=((NZ, 1, SEQS), F32),
            sq_tp=((NTP, 1, SEQS), F32),
            sq_x=((NX, 1, SEQS), F32),
            factor=((1, SEQS), F32),
            gate=((FEAT, NZ * CUT), BF16),
            up=((FEAT, NZ * CUT), BF16),
            down=((NZ * CUT, FEAT), BF16),
            gate_t=((NZ * CUT, FEAT), BF16),
            up_t=((NZ * CUT, FEAT), BF16),
            both=((2 * CUT, DEPTH), BF16),
            down_parts=((NZ, CUT, FEAT), BF16),
            down_t=((NZ, FEAT, CUT), BF16),
            sums=((2 * CUT, SEQS), BF16),
            sums_x=((NX, 2 * CUT, XS), BF16),
            hidden=((CUT, SEQS), BF16),
            outs=((NZ, NY, NC, OWN, SEQS), BF16),
            other=((NZ, NY, OWN, SEQS), BF16),
            by_y=((NY, NZ, OWN, SEQS), BF16),
            arrived_y=((NY, NZ, OWN, SEQS), BF16),
            by_z=((NZ, OWN, SEQS), BF16),
            arrived_z=((NZ, OWN, SEQS), BF16),
        ).items()
    }


SCRATCH = dict(
    ff_scratch("a_"),
    **ff_scratch("b_"),
    gate_in=((FEAT, PER * HEAD), BF16),
    value_in=((FEAT, PER * HEAD), BF16),
    write_in=((FEAT, STATE), BF16),
    read_in=((FEAT, STATE), BF16),
    out_weight=((PER * HEAD, FEAT), BF16),
    state=((ROWS, PER, HEAD, STATE), F32),
    conv=((3, ROWS, PER * HEAD + 2 * STATE), BF16),
    mix_t=((NZ, MIX, FEAT), BF16),
    mix_in=((MIX, DEPTH), BF16),
    mix_feats=((NZ, NTP, OWN, SEQS), BF16),
    mix_sq_z=((NZ, 1, SEQS), F32),
    mix_sq_tp=((NTP, 1, SEQS), F32),
    turned=((WIDE, SEQS), F32),
    rows=((NKV, ROWS, WIDE), BF16),
    rows_in=((NKV, ROWS, WIDE), BF16),
    mixed_all=((NZ, NX, ROWS, PER * HEAD), BF16),
    out_t=((NTP, OWN, SEQS), BF16),
    out_in=((NTP, OWN, SEQS), BF16),
)
STAGED = (
    "a_gate",
    "a_up",
    "a_down",
    "gate_in",
    "value_in",
    "write_in",
    "read_in",
    "b_down",
    "b_gate",
    "b_up",
    "state",
    "conv",
    "out_weight",
)
COPIES = 520


def part_of(scratch, name):
    return {key[len(name) :]: ref for key, ref in scratch.items() if key.startswith(name)}


def turn_mixer(s, step_in):
    mix_t = s["mix_t"]
    for j in range(PER * HEAD // 128):
        for ref, at in ((s["gate_in"], 0), (s["value_in"], HEAD)):
            tile = ref[:, j * 128 : (j + 1) * 128].T
            mix_t[2 * j, at : at + HEAD] = tile[:HEAD]
            mix_t[2 * j + 1, at : at + HEAD] = tile[HEAD:]
    for ref, base in ((s["write_in"], 0), (s["read_in"], 4)):
        tile = ref[...].T
        for j in range(4):
            mix_t[base + j, 2 * HEAD : 2 * HEAD + 32] = tile[32 * j : 32 * (j + 1)]
    steps = jnp.concatenate([step_in[...].astype(F32), jnp.zeros((8, FEAT), F32)], axis=0).astype(BF16)
    for j in range(NZ):
        mix_t[j, 2 * HEAD + 32 : MIX] = steps


def silu(v):
    return v / (1.0 + jnp.exp(-v))


def state_step(s, conv_weight, step_bias, log_decay_rate, group_gain, conv_next, decay_out, drive_out, write_out, ready):
    rows_in = s["rows_in"]
    parts = [sum(rows_in[k * NX + p].astype(F32) for p in range(NX)) for k in range(NZ)]
    factor = lax.rsqrt(parts[3][:, 2 * HEAD + 8 : 2 * HEAD + 9] / D + norm_epsilon)
    parts = [(part * factor).astype(BF16).astype(F32) for part in parts]
    lane = lax.broadcasted_iota(jnp.int32, (ROWS, 128), 1)
    low = lane < HEAD
    gates, values, writes, reads = [], [], 0.0, 0.0
    for j in range(PER // 2):
        a, b = parts[2 * j][:, :128], parts[2 * j + 1][:, :128]
        gates.append(jnp.where(low, a, pltpu.roll(b, HEAD, 1)))
        values.append(jnp.where(low, pltpu.roll(a, HEAD, 1), b))
    for k in range(4):
        here = lane // 32 == k
        writes = writes + jnp.where(here, parts[k][:, 128:], 0.0)
        reads = reads + jnp.where(here, parts[4 + k][:, 128:], 0.0)
    gate = jnp.concatenate(gates, axis=1)
    fresh = jnp.concatenate([*values, writes, reads], axis=1)
    ready()
    conv = s["conv"]
    conv_next[0] = conv[1]
    conv_next[1] = conv[2]
    conv_next[2] = fresh.astype(BF16)
    total = fresh * conv_weight[3]
    for t in range(3):
        total = total + conv[t].astype(F32) * conv_weight[t]
    activated = silu(total)
    inputs = activated[:, : PER * HEAD]
    write_vec = activated[:, PER * HEAD : PER * HEAD + STATE]
    read_vec = activated[:, PER * HEAD + STATE :]
    raw_step = parts[3][:, 128 : 128 + PER] + step_bias[...]
    step_size = jnp.maximum(raw_step, 0.0) + jnp.log1p(jnp.exp(-jnp.abs(raw_step)))
    decay = jnp.exp(-step_size * jnp.exp(log_decay_rate[...]))

    def over_heads(v):
        return jnp.concatenate(
            [jnp.where(low, v[:, 2 * j : 2 * j + 1], v[:, 2 * j + 1 : 2 * j + 2]) for j in range(PER // 2)],
            axis=1,
        )

    drive = over_heads(step_size) * inputs
    decay_out[...] = decay
    drive_out[...] = drive
    write_out[...] = write_vec
    row = lax.broadcasted_iota(jnp.int32, (ROWS, STATE), 0)
    state = s["state"]
    carried = 0.0
    for b in range(ROWS):
        one = jnp.where(row == b, read_vec, 0.0).astype(BF16)
        flat = state[b].reshape(PER * HEAD, STATE).astype(BF16)
        carried = carried + lax.dot_general(one, flat, (((1,), (1,)), ((), ())), preferred_element_type=F32)
    readout = over_heads(decay) * carried + drive * jnp.sum(write_vec * read_vec, axis=1, keepdims=True)
    gated = readout * silu(gate)
    scale = lax.rsqrt(jnp.mean(gated * gated, axis=1, keepdims=True) + norm_epsilon)
    return (gated * scale * group_gain[...]).astype(BF16)


def layer(*refs):
    (stream, gain_1, gain_2, gain_3, step_in, conv_weight, step_bias, log_decay_rate, group_gain) = refs[:9]
    held = dict(zip(STAGED, refs[9 : 9 + len(STAGED)]))
    refs = refs[9 + len(STAGED) :]
    result, conv_next, decay_out, drive_out, write_out = refs[:5]
    refs = refs[5:]
    s = dict(zip(SCRATCH, refs))
    sends, recvs, row_sends, row_recvs, stage_sems = refs[len(SCRATCH) :]
    wire = Wire(sends, recvs)
    z, x, kv, tp = wire.z, wire.x, wire.kv, wire.tp
    wait_greeting = greet(wire)

    staging = {
        name: pltpu.make_async_copy(held[name], s[name], stage_sems.at[i]) for i, name in enumerate(STAGED)
    }
    for copy in staging.values():
        copy.start()
    a, b = part_of(s, "a_"), part_of(s, "b_")
    staging["a_gate"].wait()
    turn_columns(a["gate"], a["gate_t"])
    staging["a_up"].wait()
    turn_columns(a["up"], a["up_t"])
    wait_greeting()
    numbers = {}

    def weights_out():
        numbers["gate"] = send_turned(wire, a["gate_t"], a["both"], 0)
        numbers["up"] = send_turned(wire, a["up_t"], a["both"], CUT)
        staging["a_down"].wait()
        numbers["down"] = send_down(wire, a["down"], a["down_parts"])
        for name in ("gate_in", "value_in", "write_in", "read_in"):
            staging[name].wait()
        turn_mixer(s, step_in)
        lanes = at_rows(z, FEAT, FEAT)
        numbers["mix"] = wire.to_z(lambda peer: s["mix_t"].at[peer], s["mix_in"].at[:, lanes])
        s["mix_in"][:, lanes] = s["mix_t"][z]

    def first_weights():
        staging["b_gate"].wait()
        turn_columns(b["gate"], b["gate_t"])
        staging["b_up"].wait()
        turn_columns(b["up"], b["up_t"])
        wait_turned(wire, numbers["gate"], a["both"], 0)
        wait_turned(wire, numbers["up"], a["both"], CUT)

    branch = channel_mixer(
        wire,
        stream[...],
        gain_1,
        a,
        weights_out,
        first_weights,
        lambda: wait_down(wire, numbers["down"], a["down_parts"], a["down_t"]),
        a["down_t"],
    )
    after = (stream[...].astype(F32) + 0.5 * branch).astype(BF16)

    def next_down():
        staging["b_down"].wait()
        numbers["next_down"] = send_down(wire, b["down"], b["down_parts"])

    squares = gather_features(wire, after, gain_2, s["mix_feats"], s["mix_sq_z"], s["mix_sq_tp"], next_down)
    wire.from_z(numbers["mix"], lambda p: s["mix_in"].at[:, at_rows(p, FEAT, FEAT)])
    part = jnp.dot(s["mix_in"][...], s["mix_feats"][...].reshape(DEPTH, SEQS), preferred_element_type=F32)
    turned = s["turned"]
    turned[2 * HEAD :, :] = jnp.zeros((WIDE - 2 * HEAD, SEQS), F32)
    turned[: 2 * HEAD, :] = part[: 2 * HEAD]
    quarter = lax.rem(z, 4)
    turned[pl.ds(pl.multiple_of(128 + 32 * quarter, 32), 32), :] = part[2 * HEAD : 2 * HEAD + 32]
    beside = pl.multiple_of(128 + 32 * lax.rem(z + 1, 4), 32)
    turned[pl.ds(beside, 8), :] = part[2 * HEAD + 32 : 2 * HEAD + 40]
    turned[pl.ds(pl.multiple_of(beside + 8, 8), 8), :] = jnp.broadcast_to(squares, (8, SEQS))
    rows, rows_in = s["rows"], s["rows_in"]
    rows[...] = turned[...].T.astype(BF16).reshape(NKV, ROWS, WIDE)

    def row_copy(d, peer, slot):
        return pltpu.make_async_remote_copy(
            src_ref=rows.at[peer],
            dst_ref=rows_in.at[slot],
            send_sem=row_sends.at[d],
            recv_sem=row_recvs.at[d],
            device_id=(peer, tp),
            device_id_type=MESH,
        )

    @pl.loop(1, NKV)
    def _(d):
        row_copy(d, lax.rem(kv + d, NKV), kv).start()

    rows_in[kv] = rows[kv]
    numbers["next_gate"] = send_turned(wire, b["gate_t"], b["both"], 0)
    staging["state"].wait()

    @pl.loop(1, NKV)
    def _(d):
        peer = lax.rem(kv + NKV - d, NKV)
        row_copy(d, peer, peer).wait_recv()

    mixed = state_step(
        s,
        conv_weight,
        step_bias,
        log_decay_rate,
        group_gain,
        conv_next,
        decay_out,
        drive_out,
        write_out,
        lambda: staging["conv"].wait(),
    )

    mixed_all = s["mixed_all"]
    mixed_all[z, x] = mixed
    own = mixed_all.at[z, x]
    n_z, n_x = {}, {}
    for d in Z_NEAR:
        n_z[d] = wire.send(own, own, wire.along_z(d) * NX + x, tp)
    n_x[0] = wire.to_x(lambda peer: own, own)
    numbers["next_up"] = send_turned(wire, b["up_t"], b["both"], CUT)
    staging["out_weight"].wait()
    steps = [(0, z)] + [(d, wire.along_z(NZ - d)) for d in Z_NEAR]
    for d, peer in steps[1:]:
        block = mixed_all.at[peer, x]
        wire.recv(n_z[d], block, peer * NX + x, tp)
        n_x[d] = wire.to_x(lambda p, block=block: block, block)
    for d, peer in steps:
        wire.from_x(n_x[d], lambda p, peer=peer: mixed_all.at[peer, p])
    part = jnp.dot(mixed_all[...].reshape(SEQS, PER * HEAD), s["out_weight"][...], preferred_element_type=F32)
    out_t, out_in = s["out_t"], s["out_in"]
    out_t[...] = part.T.astype(BF16).reshape(NTP, OWN, SEQS)
    n_tp = wire.to_tp(lambda peer: out_t.at[peer], out_in.at[tp])
    out_in[tp] = out_t[tp]
    wire.from_tp(n_tp, lambda p: out_in.at[p])
    after = (after.astype(F32) + jnp.sum(out_in[...].astype(F32), axis=0)).astype(BF16)

    def second_weights():
        wait_turned(wire, numbers["next_gate"], b["both"], 0)
        wait_turned(wire, numbers["next_up"], b["both"], CUT)

    branch = channel_mixer(
        wire,
        after,
        gain_3,
        b,
        lambda: wait_down(wire, numbers["next_down"], b["down_parts"], b["down_t"]),
        second_weights,
        lambda: None,
        b["down_t"],
    )
    result[...] = (after.astype(F32) + 0.5 * branch).astype(BF16)
    wire.drain()

    @pl.loop(1, NKV)
    def _(d):
        row_copy(d, lax.rem(kv + d, NKV), kv).wait_send()


def on_device(
    stream,
    ssm_state,
    conv_state,
    first_gain,
    first_gate,
    first_up,
    first_down,
    mix_gain,
    gate_in,
    value_in,
    write_in,
    read_in,
    step_in,
    conv_weight,
    step_bias,
    log_decay_rate,
    group_gain,
    out_weight,
    last_norm_gain,
    second_gate,
    second_up,
    second_down,
):
    staged = dict(
        a_gate=first_gate,
        a_up=first_up,
        a_down=first_down,
        gate_in=gate_in,
        value_in=value_in,
        write_in=write_in,
        read_in=read_in,
        b_down=second_down,
        b_gate=second_gate,
        b_up=second_up,
        state=ssm_state,
        conv=conv_state[:, :, 0].transpose(1, 0, 2),
        out_weight=out_weight,
    )
    small = (
        stream.T,
        first_gain[None],
        mix_gain[None],
        last_norm_gain[None],
        step_in.T,
        conv_weight,
        step_bias[None],
        log_decay_rate[None],
        group_gain[None],
    )
    whole = pl.BlockSpec(memory_space=pltpu.VMEM)
    outs = (
        jax.ShapeDtypeStruct((OWN, SEQS), BF16),
        jax.ShapeDtypeStruct((3, ROWS, PER * HEAD + 2 * STATE), BF16),
        jax.ShapeDtypeStruct((ROWS, PER), F32),
        jax.ShapeDtypeStruct((ROWS, PER * HEAD), F32),
        jax.ShapeDtypeStruct((ROWS, STATE), F32),
    )
    result, conv_next, decay, drive, write_vec = pl.pallas_call(
        layer,
        name="layer",
        out_shape=outs,
        in_specs=[whole] * len(small) + [pl.BlockSpec(memory_space=pl.ANY)] * len(STAGED),
        out_specs=[whole] * len(outs),
        scratch_shapes=[pltpu.VMEM(shape, dtype) for shape, dtype in SCRATCH.values()]
        + [pltpu.SemaphoreType.DMA((COPIES,))] * 2
        + [pltpu.SemaphoreType.DMA((NKV,))] * 2
        + [pltpu.SemaphoreType.DMA((len(STAGED),))],
        compiler_params=pltpu.CompilerParams(
            collective_id=0, has_side_effects=True, vmem_limit_bytes=60 * 1024 * 1024
        ),
    )(*small, *(staged[name] for name in STAGED))
    ssm_next = (
        ssm_state * decay[:, :, None, None]
        + drive.reshape(ROWS, PER, HEAD)[..., None] * write_vec[:, None, None, :]
    )
    return (result.T, ssm_next, conv_next.transpose(1, 0, 2)[:, :, None])


def solution(mesh):
    placed = (
        P(None, ("kv", "tp")),
        P("kv", "tp", None, None),
        P("kv", None, "tp", None),
        P(("kv", "tp")),
        P("kv", "tp"),
        P("kv", "tp"),
        P("tp", "kv"),
        P(("kv", "tp")),
        P("kv", "tp"),
        P("kv", "tp"),
        P("kv", "tp"),
        P("kv", "tp"),
        P("kv", "tp"),
        P(None, "tp", None),
        P("tp"),
        P("tp"),
        P("tp"),
        P("tp", "kv"),
        P(("kv", "tp")),
        P("kv", "tp"),
        P("kv", "tp"),
        P("tp", "kv"),
    )
    return jax.shard_map(
        on_device,
        mesh=mesh,
        in_specs=placed,
        out_specs=(P(None, ("kv", "tp")), P("kv", "tp", None, None), P("kv", None, "tp", None)),
        check_vma=False,
    )
```

time: 180 us -> 155 us (0.86)
  local copies, waits for them, and re-layouts: 14.9 us -> 2.08 us
  Pallas kernels: 156 us -> 148 us
    unnamed x34 -> x6, local copies, waits for them, and re-layouts: 11.3 us -> 1.25 us
    pallas_call x2 -> x1, Pallas kernels: 156 us -> 148 us  [on_device(): pl.pallas_call(layer, name='layer', out_shape=outs, in_specs=[whole] * le...]
where the time goes in v2:
time: 155 us
  Pallas kernels  148 us (95%)
  other arithmetic  4.4 us (3%)
  local copies, waits for them, and re-layouts  2.08 us (1%)
    pallas_call x1, Pallas kernels, on_device(): pl.pallas_call(layer, name='layer', out_shape=outs, in_specs=[whole] * le...  148 us
    add x1, other arithmetic, on_device(): ssm_state * decay[:, :, None, None]  4.4 us

profile of v2, /device:TPU:1, one launch (start us, length us, event | category | flops | bytes accessed | tf_op | source)
XLA Modules:
  0.0 155.0 jit_solution(17393876929955501455)
XLA Ops:
  0.6 147.9 %layer.1 = (bf16[16,512]{1,0:T(8,128)(2,1)}, bf16[3,16,768]{2,1,0:T(8,128)(2,1)}, f32[16,8]{1,0:T(8,128)}, f32[16,512]{1,0:T(8,128)}, f32[16,128]{1,0:T(8,128)}) custom-call(bf16[16,512]{1,0:T(8,128)(2,1)} %bitcast.19, f32[1,16]{1,0:T(1,128)} %bitcast.23, f32[1,16]{1,0:T(1,128)} %bitcast.24, f32[1,16]{1,0:T(1,128)} %bitcast.25, bf16[8,128]{1,0:T(8,128)(2,1)} %bitcast.21, ...), custom_call_target="tpu_custom_call" | custom-call | tf_op jit(solution)/shard_map/layer/pallas_call | solution.py:645
  148.5 0.8 mul.25
  149.4 0.0 copy-start.1
  149.4 0.0 copy-start
  149.4 4.4 %multiply_add_fusion = f32[16,8,64,128]{3,2,1,0:T(8,128)} fusion(f32[16,8,64,128]{3,2,1,0:T(8,128)} %refs_19_.1, f32[16,128]{1,0:T(8,128)} %get-tuple-element.11, f32[16,8,64]{2,1,0:T(8,128)S(1)} %mul.25, f32[16,8]{1,0:T(8,128)} %get-tuple-element.9), kind=kLoop, calls=%fused_computation | loop fusion | flops 3145728 | bytes 8430080 | tf_op jit(solution)/shard_map/add | solution.py:660
  153.8 0.0 copy-done.1
  153.8 0.6 copy.28
  154.4 0.0 copy-done
  154.4 0.6 copy.29
Async XLA Ops:
  149.4 4.4 %copy-start.1 = (bf16[16,512]{1,0:T(8,128)(2,1)S(1)}, bf16[16,512]{1,0:T(8,128)(2,1)}, u32[]{:S(2)}) copy-start(bf16[16,512]{1,0:T(8,128)(2,1)} %get-tuple-element.8) | copy-start | bytes 49156
  149.4 5.0 %copy-start = (bf16[3,16,768]{2,1,0:T(8,128)(2,1)S(1)}, bf16[3,16,768]{2,1,0:T(8,128)(2,1)}, u32[]{:S(2)}) copy-start(bf16[3,16,768]{2,1,0:T(8,128)(2,1)} %get-tuple-element.12) | copy-start | bytes 221188

commit v3 on v2

v3 whole, which is shorter than its diff:
```python
import jax
import jax.numpy as jnp
from jax import lax
from jax.experimental import pallas as pl
from jax.experimental.pallas import tpu as pltpu
from jax.sharding import PartitionSpec as P

MESH = pl.DeviceIdType.MESH
F32, BF16 = jnp.float32, jnp.bfloat16

NZ, NX, NY, NC = 8, 4, 4, 2
NKV, NTP = NZ * NX, NY * NC
SEQS, D, FF = 512, 4096, 11264
OWN = D // (NKV * NTP)
FEAT = OWN * NTP
DEPTH = FEAT * NZ
CUT = FF // NTP // NZ
XS = SEQS // NX
ROWS = SEQS // NKV
HEAD, STATE, PER = 64, 128, 8
MIX = 176
WIDE = 256
PARTS = ((0, 96), (96, 80))
norm_epsilon = 1e-06


class Wire:
    def __init__(self, sends, recvs):
        self.sends, self.recvs, self.n_sends, self.n_recvs, self.pending = sends, recvs, 0, 0, []
        kv, self.tp = lax.axis_index("kv"), lax.axis_index("tp")
        self.kv = kv
        self.z, self.x = lax.div(kv, NX), lax.rem(kv, NX)
        self.y, self.c = lax.div(self.tp, NC), lax.rem(self.tp, NC)
        self.sibling = self.y * NC + (1 - self.c)

    def along_y(self, d):
        return lax.rem(self.y + d, NY)

    def along_tp(self, d):
        return lax.rem(self.tp + d, NTP)

    def settle(self, keep=()):
        for copies in self.pending:
            if copies not in keep:
                copies.left()
        self.pending = [copies for copies in self.pending if copies in keep]


class Copies:
    def __init__(self, wire, every, pending=True):
        self.wire, self.every, self.keys = wire, every, {}
        self.sem = wire.sends.at[wire.n_sends]
        wire.n_sends += 1
        if pending:
            wire.pending.append(self)

    def arrival(self, key):
        if key not in self.keys:
            self.keys[key] = self.wire.n_recvs
            self.wire.n_recvs += 1
        return self.wire.recvs.at[self.keys[key]]

    def _copy(self, src, dst, kv, tp, key):
        return pltpu.make_async_remote_copy(
            src_ref=src,
            dst_ref=dst,
            send_sem=self.sem,
            recv_sem=self.arrival(key),
            device_id=(kv, tp),
            device_id_type=MESH,
        )

    def send(self, src, dst, kv, tp, key=0):
        self._copy(src, dst, kv, tp, key).start()

    def arrived(self, whole, key=0):
        self._copy(whole, whole, self.wire.kv, self.wire.sibling, key).wait_recv()

    def left(self):
        self._copy(self.every, self.every, self.wire.kv, self.wire.sibling, next(iter(self.keys))).wait_send()

    def to_y(self, src, dst, key=0):
        wire = self.wire
        for d in (2, 1, 3):
            peer = wire.along_y(d)
            self.send(src(peer), dst, wire.kv, peer * NC + wire.c, key)

    def to_tp(self, src, dst):
        for d in range(1, NTP):
            peer = self.wire.along_tp(d)
            self.send(src(peer), dst, self.wire.kv, peer)

    def to_g(self, plane, src, dst):
        for d in plane.far:
            peer = plane.ahead(d)
            self.send(src(peer), dst, plane.kv_at(peer, plane.h), self.wire.tp)

    def to_h(self, plane, src, dst, key=0):
        for d in (2, 1, 3):
            peer = lax.rem(plane.h + d, NX)
            self.send(src(peer), dst, plane.kv_at(plane.g, peer), self.wire.tp, key)


class Plane:
    def __init__(self, wire, folded):
        self.folded = folded
        if folded:
            self.g, self.h = wire.x + NX * lax.rem(wire.z, 2), lax.div(wire.z, 2)
            self.near = (1, 3, 4, 5, 7, 2, 6)
        else:
            self.g, self.h = wire.z, wire.x
            self.near = (1, 7, 2, 6, 3, 5, 4)
        self.far = self.near[::-1]

    def kv_at(self, g, h):
        if self.folded:
            if isinstance(g, int) and isinstance(h, int):
                return (2 * h + g // NX) * NX + g % NX
            return (2 * h + lax.div(g, NX)) * NX + lax.rem(g, NX)
        return g * NX + h

    def ahead(self, d):
        if not self.folded:
            return lax.rem(self.g + d, NZ)
        x, pair = lax.rem(self.g, NX), lax.div(self.g, NX)
        return lax.rem(x + d % NX, NX) + NX * lax.rem(pair + d // NX, 2)

    def behind(self, d):
        if not self.folded:
            return lax.rem(self.g + NZ - d, NZ)
        x, pair = lax.rem(self.g, NX), lax.div(self.g, NX)
        return lax.rem(x + NX - d % NX, NX) + NX * lax.rem(pair + d // NX, 2)


def greet(wire):
    barrier = pltpu.get_barrier_semaphore()

    def tell(kv, tp):
        pl.semaphore_signal(barrier, inc=1, device_id=(kv, tp), device_id_type=MESH)

    for d in range(1, NZ):
        tell(lax.rem(wire.z + d, NZ) * NX + wire.x, wire.tp)
    for d in range(1, NX):
        x = lax.rem(wire.x + d, NX)
        tell(wire.z * NX + x, wire.tp)
        tell((wire.z + 1 - 2 * lax.rem(wire.z, 2)) * NX + x, wire.tp)
    for d in range(1, NTP):
        tell(wire.kv, wire.along_tp(d))
    return lambda: pl.semaphore_wait(barrier, NZ - 1 + 2 * (NX - 1) + NTP - 1)


def at_rows(start, size, step):
    return pl.ds(pl.multiple_of(start * step, step), size)


def turn_columns(src, dst):
    for j in range(src.shape[1] // 128):
        dst[j * 128 : (j + 1) * 128, :] = src[:, j * 128 : (j + 1) * 128].T


def send_gate_up(wire, plane, gate_t, up_t, both, part):
    g = plane.g
    lanes = at_rows(g, FEAT, FEAT)
    start, size = PARTS[part]
    out = []
    for turned, at in ((gate_t, 2 * start), (up_t, 2 * start + size)):
        copies = Copies(wire, both.at[at : at + size, 0 : (NZ - 1) * FEAT], False)

        def cut(peer):
            return pl.ds(pl.multiple_of(peer * CUT + start, OWN), size)

        copies.to_g(plane, lambda peer: turned.at[cut(peer), :], both.at[at : at + size, lanes])
        both[at : at + size, lanes] = turned[cut(g), :]
        out.append(copies)
    return out


def wait_all(sets):
    for copies in sets:
        copies.arrived(copies.every)


def send_down(wire, plane, down, parts):
    g = plane.g
    copies = Copies(wire, parts.at[0 : NZ - 1], False)
    copies.to_g(plane, lambda peer: down.at[at_rows(peer, CUT, CUT), :], parts.at[g])
    parts[g] = down[at_rows(g, CUT, CUT), :]
    return copies


def wait_down(copies, parts, turned):
    copies.arrived(copies.every)
    for s in range(NZ):
        turned[s] = parts[s].T


def silu(v):
    return v / (1.0 + jnp.exp(-v))


def as_column(row):
    square = jnp.broadcast_to(row, (OWN, OWN))
    same = lax.broadcasted_iota(jnp.int32, (OWN, OWN), 0) == lax.broadcasted_iota(jnp.int32, (OWN, OWN), 1)
    return jnp.sum(jnp.where(same, square, 0.0), axis=1, keepdims=True)


def gather_features(wire, plane, values, gain, feats, sq_g, sq_tp, after_first_sends):
    g, tp, c, sibling = plane.g, wire.tp, wire.c, wire.sibling
    wide = values.astype(F32)
    feats[g, tp] = (wide * as_column(gain[...])).astype(BF16)
    own = feats.at[g, tp]
    to_group = Copies(wire, feats.at[0, 0 : NZ - 1])
    for d in plane.near:
        to_group.send(own, own, plane.kv_at(plane.ahead(d), plane.h), tp, d)
    along = Copies(wire, feats.at[0 : NY - 1])
    across = Copies(wire, feats.at[0:NY])

    def hand_on(d, peer):
        block = feats.at[peer, tp]
        along.to_y(lambda p: block, block, d)
        across.send(block, block, wire.kv, sibling)

    hand_on(0, g)
    sq_g[g] = jnp.sum(wide * wide, axis=0, keepdims=True)
    squares_g = Copies(wire, sq_g.at[0 : NZ - 1])
    squares_g.to_g(plane, lambda peer: sq_g.at[g], sq_g.at[g])
    after_first_sends()
    steps = [(0, g)] + [(d, plane.behind(d)) for d in plane.near]
    for d, peer in steps[1:]:
        to_group.arrived(feats.at[peer, tp], d)
        hand_on(d, peer)
    squares_g.arrived(squares_g.every)
    sq_tp[tp] = jnp.sum(sq_g[...], axis=0)
    squares_tp = Copies(wire, sq_tp.at[0 : NTP - 1])
    squares_tp.to_tp(lambda peer: sq_tp.at[tp], sq_tp.at[tp])
    for d, peer in steps:
        along.arrived(feats.at[peer, 0 : NY - 1], d)
        for e in (1, 3, 2):
            block = feats.at[peer, wire.along_y(NY - e) * NC + c]
            across.send(block, block, wire.kv, sibling)
    squares_tp.arrived(squares_tp.every)
    across.arrived(across.every)
    return jnp.sum(sq_tp[...], axis=0)


def channel_mixer(wire, plane, values, gain, s, after_first_sends, wait_weights, after_hidden, down_t):
    g, h = plane.g, plane.h
    squares = gather_features(wire, plane, values, gain, s["feats"], s["sq_g"], s["sq_tp"], after_first_sends)
    sq_h, sums, sums_h, hidden = s["sq_h"], s["sums"], s["sums_h"], s["hidden"]
    sq_h[h] = squares
    squares_h = Copies(wire, sq_h.at[0 : NX - 1])
    squares_h.to_h(plane, lambda peer: sq_h.at[h], sq_h.at[h])
    gathered = list(wire.pending)
    sums_out = []
    for part, (start, size) in enumerate(PARTS):
        wait_weights(part)
        rows = slice(2 * start, 2 * (start + size))
        sums[rows] = jnp.dot(
            s["both"][rows], s["feats"][...].reshape(DEPTH, SEQS), preferred_element_type=F32
        ).astype(BF16)
        copies = Copies(wire, sums_h.at[0 : NX - 1, rows])
        copies.to_h(plane, lambda peer: sums.at[rows, at_rows(peer, XS, XS)], sums_h.at[h, rows])
        sums_h[h, rows] = sums[rows, at_rows(h, XS, XS)]
        sums_out.append(copies)
    squares_h.arrived(squares_h.every)
    s["factor"][...] = lax.rsqrt(jnp.sum(sq_h[...], axis=0) / D + norm_epsilon)
    factor = s["factor"][:, at_rows(h, XS, XS)]
    hidden_out = []
    for (start, size), copies in zip(PARTS, sums_out):
        copies.arrived(copies.every)
        at = 2 * start
        gates = sum(sums_h[p, at : at + size].astype(F32) for p in range(NX)) * factor
        ups = sum(sums_h[p, at + size : at + 2 * size].astype(F32) for p in range(NX)) * factor
        here = hidden.at[start : start + size, at_rows(h, XS, XS)]
        here[...] = (silu(gates) * ups).astype(BF16)
        out = Copies(wire, hidden.at[start : start + size, 0 : SEQS - XS])
        out.to_h(plane, lambda peer: here, here)
        hidden_out.append(out)
    after_hidden()
    for copies in gathered:
        copies.left()
    wire.pending = [copies for copies in wire.pending if copies not in gathered]
    wait_all(hidden_out)

    c, y = wire.c, wire.y
    outs, other = s["outs"], s["other"]
    by_y, arrived_y = s["by_y"], s["arrived_y"]
    by_g, arrived_g = s["by_g"], s["arrived_g"]
    order = [(d, plane.ahead(d)) for d in plane.far + (0,)]
    across, along = Copies(wire, other), Copies(wire, by_y.at[0 : NY - 1])
    to_group = Copies(wire, by_g.at[0 : NZ - 1])
    for d, k in order:
        part = jnp.dot(down_t[k], hidden[...], preferred_element_type=F32)
        outs[k] = part.astype(BF16).reshape(NY, NC, OWN, SEQS)
        across.send(outs.at[k, :, 1 - c], other.at[k], wire.kv, wire.sibling, d)
    for d, k in order:
        across.arrived(other.at[k], d)
        by_y[:, k] = (outs[k, :, c].astype(F32) + other[k].astype(F32)).astype(BF16)
        along.to_y(lambda peer: by_y.at[peer, k], arrived_y.at[y, k], d)
        arrived_y[y, k] = by_y[y, k]
    for d, k in order:
        along.arrived(arrived_y.at[0 : NY - 1, k], d)
        by_g[k] = sum(arrived_y[p, k].astype(F32) for p in range(NY)).astype(BF16)
        if d:
            to_group.send(by_g.at[k], arrived_g.at[g], plane.kv_at(k, h), wire.tp)
    arrived_g[g] = by_g[g]
    wire.settle((to_group,))
    to_group.arrived(to_group.every)
    return jnp.sum(arrived_g[...].astype(F32), axis=0)


def ff_scratch(name):
    return {
        name + key: value
        for key, value in dict(
            feats=((NZ, NTP, OWN, SEQS), BF16),
            sq_g=((NZ, 1, SEQS), F32),
            sq_tp=((NTP, 1, SEQS), F32),
            sq_h=((NX, 1, SEQS), F32),
            factor=((1, SEQS), F32),
            gate=((FEAT, NZ * CUT), BF16),
            up=((FEAT, NZ * CUT), BF16),
            down=((NZ * CUT, FEAT), BF16),
            gate_t=((NZ * CUT, FEAT), BF16),
            up_t=((NZ * CUT, FEAT), BF16),
            both=((2 * CUT, DEPTH), BF16),
            down_parts=((NZ, CUT, FEAT), BF16),
            down_t=((NZ, FEAT, CUT), BF16),
            sums=((2 * CUT, SEQS), BF16),
            sums_h=((NX, 2 * CUT, XS), BF16),
            hidden=((CUT, SEQS), BF16),
            outs=((NZ, NY, NC, OWN, SEQS), BF16),
            other=((NZ, NY, OWN, SEQS), BF16),
            by_y=((NY, NZ, OWN, SEQS), BF16),
            arrived_y=((NY, NZ, OWN, SEQS), BF16),
            by_g=((NZ, OWN, SEQS), BF16),
            arrived_g=((NZ, OWN, SEQS), BF16),
        ).items()
    }


SCRATCH = dict(
    ff_scratch("a_"),
    **ff_scratch("b_"),
    gate_in=((FEAT, PER * HEAD), BF16),
    value_in=((FEAT, PER * HEAD), BF16),
    write_in=((FEAT, STATE), BF16),
    read_in=((FEAT, STATE), BF16),
    out_weight=((PER * HEAD, FEAT), BF16),
    state=((ROWS, PER, HEAD, STATE), F32),
    conv=((3, ROWS, PER * HEAD + 2 * STATE), BF16),
    mix_t=((NZ, MIX, FEAT), BF16),
    mix_in=((MIX, DEPTH), BF16),
    mix_feats=((NZ, NTP, OWN, SEQS), BF16),
    mix_sq_g=((NZ, 1, SEQS), F32),
    mix_sq_tp=((NTP, 1, SEQS), F32),
    turned=((WIDE, SEQS), F32),
    rows=((NKV, ROWS, WIDE), BF16),
    rows_in=((NKV, ROWS, WIDE), BF16),
    mixed_all=((NZ, NX, ROWS, PER * HEAD), BF16),
    out_t=((NTP, OWN, SEQS), BF16),
    out_in=((NTP, OWN, SEQS), BF16),
)
STAGED = (
    "a_gate",
    "a_up",
    "a_down",
    "gate_in",
    "value_in",
    "write_in",
    "read_in",
    "b_down",
    "b_gate",
    "b_up",
    "state",
    "conv",
    "out_weight",
)
LEAVE, ARRIVE = 56, 136
VMEM_LIMIT = 58 * 1024 * 1024


def part_of(scratch, name):
    return {key[len(name) :]: ref for key, ref in scratch.items() if key.startswith(name)}


def turn_mixer(s, step_in):
    mix_t = s["mix_t"]
    for j in range(PER * HEAD // 128):
        for ref, at in ((s["gate_in"], 0), (s["value_in"], HEAD)):
            tile = ref[:, j * 128 : (j + 1) * 128].T
            mix_t[2 * j, at : at + HEAD] = tile[:HEAD]
            mix_t[2 * j + 1, at : at + HEAD] = tile[HEAD:]
    for ref, base in ((s["write_in"], 0), (s["read_in"], 4)):
        tile = ref[...].T
        for j in range(4):
            mix_t[base + j, 2 * HEAD : 2 * HEAD + 32] = tile[32 * j : 32 * (j + 1)]
    steps = jnp.concatenate([step_in[...].astype(F32), jnp.zeros((8, FEAT), F32)], axis=0).astype(BF16)
    for j in range(NZ):
        mix_t[j, 2 * HEAD + 32 : MIX] = steps


def state_step(s, plane, conv_weight, step_bias, log_decay_rate, group_gain, conv_next, state, ready):
    rows_in = s["rows_in"]
    parts = [sum(rows_in[plane.kv_at(k, p)].astype(F32) for p in range(NX)) for k in range(NZ)]
    factor = lax.rsqrt(parts[3][:, 2 * HEAD + 8 : 2 * HEAD + 9] / D + norm_epsilon)
    parts = [(part * factor).astype(BF16).astype(F32) for part in parts]
    lane = lax.broadcasted_iota(jnp.int32, (ROWS, 128), 1)
    low = lane < HEAD
    gates, values, writes, reads = [], [], 0.0, 0.0
    for j in range(PER // 2):
        a, b = parts[2 * j][:, :128], parts[2 * j + 1][:, :128]
        gates.append(jnp.where(low, a, pltpu.roll(b, HEAD, 1)))
        values.append(jnp.where(low, pltpu.roll(a, HEAD, 1), b))
    for k in range(4):
        here = lane // 32 == k
        writes = writes + jnp.where(here, parts[k][:, 128:], 0.0)
        reads = reads + jnp.where(here, parts[4 + k][:, 128:], 0.0)
    gate = jnp.concatenate(gates, axis=1)
    fresh = jnp.concatenate([*values, writes, reads], axis=1)
    ready()
    conv = s["conv"]
    conv_next[0] = conv[1]
    conv_next[1] = conv[2]
    conv_next[2] = fresh.astype(BF16)
    total = fresh * conv_weight[3]
    for t in range(3):
        total = total + conv[t].astype(F32) * conv_weight[t]
    activated = silu(total)
    inputs = activated[:, : PER * HEAD]
    write_vec = activated[:, PER * HEAD : PER * HEAD + STATE]
    read_vec = activated[:, PER * HEAD + STATE :]
    raw_step = parts[3][:, 128 : 128 + PER] + step_bias[...]
    step_size = jnp.maximum(raw_step, 0.0) + jnp.log1p(jnp.exp(-jnp.abs(raw_step)))
    decay = jnp.exp(-step_size * jnp.exp(log_decay_rate[...]))

    def over_heads(v):
        return jnp.concatenate(
            [jnp.where(low, v[:, 2 * j : 2 * j + 1], v[:, 2 * j + 1 : 2 * j + 2]) for j in range(PER // 2)],
            axis=1,
        )

    drive, kept = over_heads(step_size) * inputs, over_heads(decay)
    row = lax.broadcasted_iota(jnp.int32, (ROWS, STATE), 0)
    carried = 0.0
    for b in range(ROWS):
        one = jnp.where(row == b, read_vec, 0.0).astype(BF16)
        flat = state[b].reshape(PER * HEAD, STATE).astype(BF16)
        carried = carried + lax.dot_general(one, flat, (((1,), (1,)), ((), ())), preferred_element_type=F32)
    readout = kept * carried + drive * jnp.sum(write_vec * read_vec, axis=1, keepdims=True)
    gated = readout * silu(gate)
    scale = lax.rsqrt(jnp.mean(gated * gated, axis=1, keepdims=True) + norm_epsilon)
    return (gated * scale * group_gain[...]).astype(BF16), (kept, drive, write_vec)


def layer(*refs):
    (stream, gain_1, gain_2, gain_3, step_in, conv_weight, step_bias, log_decay_rate, group_gain) = refs[:9]
    held = dict(zip(STAGED, refs[9 : 9 + len(STAGED)]))
    refs = refs[9 + len(STAGED) :]
    result, conv_next, kept_out, drive_out, write_out = refs[:5]
    refs = refs[5:]
    s = dict(zip(SCRATCH, refs))
    sends, recvs, stage_sems = refs[len(SCRATCH) :]
    wire = Wire(sends, recvs)
    plain, folded = Plane(wire, False), Plane(wire, True)
    z, x, kv, tp = wire.z, wire.x, wire.kv, wire.tp
    wait_greeting = greet(wire)

    staging = {
        name: pltpu.make_async_copy(held[name], s[name], stage_sems.at[i]) for i, name in enumerate(STAGED)
    }
    for copy in staging.values():
        copy.start()
    a, b = part_of(s, "a_"), part_of(s, "b_")
    staging["a_gate"].wait()
    turn_columns(a["gate"], a["gate_t"])
    staging["a_up"].wait()
    turn_columns(a["up"], a["up_t"])
    wait_greeting()
    sets = {}

    def weights_out():
        sets["first"] = [send_gate_up(wire, folded, a["gate_t"], a["up_t"], a["both"], part) for part in (0, 1)]
        staging["a_down"].wait()
        sets["down"] = send_down(wire, folded, a["down"], a["down_parts"])
        for name in ("gate_in", "value_in", "write_in", "read_in"):
            staging[name].wait()
        turn_mixer(s, step_in)

    def first_weights(part):
        if part == 0:
            staging["b_gate"].wait()
            turn_columns(b["gate"], b["gate_t"])
            staging["b_up"].wait()
            turn_columns(b["up"], b["up_t"])
        wait_all(sets["first"][part])

    def after_first_hidden():
        lanes = at_rows(folded.g, FEAT, FEAT)
        sets["mix"] = Copies(wire, s["mix_in"].at[:, 0 : (NZ - 1) * FEAT], False)
        sets["mix"].to_g(folded, lambda peer: s["mix_t"].at[peer], s["mix_in"].at[:, lanes])
        s["mix_in"][:, lanes] = s["mix_t"][folded.g]
        staging["b_down"].wait()
        sets["next_down"] = send_down(wire, plain, b["down"], b["down_parts"])
        wait_down(sets["down"], a["down_parts"], a["down_t"])

    branch = channel_mixer(
        wire, folded, stream[...], gain_1, a, weights_out, first_weights, after_first_hidden, a["down_t"]
    )
    after = (stream[...].astype(F32) + 0.5 * branch).astype(BF16)

    def next_gate():
        sets["second"] = [send_gate_up(wire, plain, b["gate_t"], b["up_t"], b["both"], 0)]

    squares = gather_features(
        wire, folded, after, gain_2, s["mix_feats"], s["mix_sq_g"], s["mix_sq_tp"], next_gate
    )
    wait_all([sets["mix"]])
    part = jnp.dot(s["mix_in"][...], s["mix_feats"][...].reshape(DEPTH, SEQS), preferred_element_type=F32)
    turned = s["turned"]
    turned[2 * HEAD :, :] = jnp.zeros((WIDE - 2 * HEAD, SEQS), F32)
    turned[: 2 * HEAD, :] = part[: 2 * HEAD]
    quarter = lax.rem(folded.g, 4)
    turned[pl.ds(pl.multiple_of(128 + 32 * quarter, 32), 32), :] = part[2 * HEAD : 2 * HEAD + 32]
    beside = pl.multiple_of(128 + 32 * lax.rem(folded.g + 1, 4), 32)
    turned[pl.ds(beside, 8), :] = part[2 * HEAD + 32 : 2 * HEAD + 40]
    turned[pl.ds(pl.multiple_of(beside + 8, 8), 8), :] = jnp.broadcast_to(squares, (8, SEQS))
    rows, rows_in = s["rows"], s["rows_in"]
    rows[...] = turned[...].T.astype(BF16).reshape(NKV, ROWS, WIDE)

    row_copies = Copies(wire, rows.at[0 : NKV - 1])
    row_copies.arrival(0)

    @pl.loop(1, NKV)
    def _(d):
        peer = lax.rem(kv + d, NKV)
        row_copies.send(rows.at[peer], rows_in.at[kv], peer, tp)

    rows_in[kv] = rows[kv]
    wire.settle((row_copies,))
    wait_down(sets["next_down"], b["down_parts"], b["down_t"])
    staging["state"].wait()
    row_copies.arrived(rows_in.at[0 : NKV - 1])
    mixed, change = state_step(
        s,
        folded,
        conv_weight,
        step_bias,
        log_decay_rate,
        group_gain,
        conv_next,
        s["state"],
        lambda: staging["conv"].wait(),
    )

    mixed_all = s["mixed_all"]
    mixed_all[z, x] = mixed
    own = mixed_all.at[z, x]
    to_z = Copies(wire, mixed_all.at[0 : NZ - 1, 0])
    to_x = Copies(wire, mixed_all.at[0 : NZ - 2])
    for d in plain.near:
        to_z.send(own, own, plain.kv_at(plain.ahead(d), x), tp, d)
    to_x.to_h(plain, lambda peer: own, own)
    sets["second"].append(send_gate_up(wire, plain, b["gate_t"], b["up_t"], b["both"], 1))
    kept_out[...], drive_out[...], write_out[...] = change
    staging["out_weight"].wait()
    wire.settle((to_z, to_x))
    for d in plain.near:
        block = mixed_all.at[plain.behind(d), x]
        to_z.arrived(block, d)
        to_x.to_h(plain, lambda peer: block, block)
    to_x.arrived(to_x.every)
    part = jnp.dot(mixed_all[...].reshape(SEQS, PER * HEAD), s["out_weight"][...], preferred_element_type=F32)
    out_t, out_in = s["out_t"], s["out_in"]
    out_t[...] = part.T.astype(BF16).reshape(NTP, OWN, SEQS)
    to_tp = Copies(wire, out_in.at[0 : NTP - 1])
    to_tp.to_tp(lambda peer: out_t.at[peer], out_in.at[tp])
    out_in[tp] = out_t[tp]
    wire.settle((to_tp,))
    to_tp.arrived(to_tp.every)
    after = (after.astype(F32) + jnp.sum(out_in[...].astype(F32), axis=0)).astype(BF16)

    def bulk_left():
        for copies in [sets["down"], sets["mix"], sets["next_down"], *sum(sets["first"] + sets["second"], [])]:
            copies.left()

    branch = channel_mixer(
        wire,
        plain,
        after,
        gain_3,
        b,
        lambda: None,
        lambda part: wait_all(sets["second"][part]),
        bulk_left,
        b["down_t"],
    )
    result[...] = (after.astype(F32) + 0.5 * branch).astype(BF16)
    wire.settle()


def finish(stream_in, conv_in, kept, drive, write_vec, state, result, conv_next, state_next, held, done, reads, writes):
    into = [pltpu.make_async_copy(state.at[b], held.at[b], reads.at[b]) for b in range(ROWS)]
    out = [pltpu.make_async_copy(done.at[b], state_next.at[b], writes.at[b]) for b in range(ROWS)]
    for copy in into:
        copy.start()
    kept_t, drive_t = kept[...].T, drive[...].T
    result[...] = stream_in[...]
    conv_next[...] = conv_in[...]
    for b in range(ROWS):
        into[b].wait()
        flat = held[b].reshape(PER * HEAD, STATE)
        new = flat * kept_t[:, b : b + 1] + drive_t[:, b : b + 1] * write_vec[b : b + 1]
        done[b] = new.reshape(PER, HEAD, STATE)
        out[b].start()
    for copy in out:
        copy.wait()


def on_device(
    stream,
    ssm_state,
    conv_state,
    first_gain,
    first_gate,
    first_up,
    first_down,
    mix_gain,
    gate_in,
    value_in,
    write_in,
    read_in,
    step_in,
    conv_weight,
    step_bias,
    log_decay_rate,
    group_gain,
    out_weight,
    last_norm_gain,
    second_gate,
    second_up,
    second_down,
):
    staged = dict(
        a_gate=first_gate,
        a_up=first_up,
        a_down=first_down,
        gate_in=gate_in,
        value_in=value_in,
        write_in=write_in,
        read_in=read_in,
        b_down=second_down,
        b_gate=second_gate,
        b_up=second_up,
        state=ssm_state,
        conv=conv_state[:, :, 0].transpose(1, 0, 2),
        out_weight=out_weight,
    )
    small = (
        stream.T,
        first_gain[None],
        mix_gain[None],
        last_norm_gain[None],
        step_in.T,
        conv_weight,
        step_bias[None],
        log_decay_rate[None],
        group_gain[None],
    )
    whole = pl.BlockSpec(memory_space=pltpu.VMEM)
    channels = PER * HEAD + 2 * STATE
    outs = (
        jax.ShapeDtypeStruct((OWN, SEQS), BF16),
        jax.ShapeDtypeStruct((3, ROWS, channels), BF16),
        jax.ShapeDtypeStruct((ROWS, PER * HEAD), F32),
        jax.ShapeDtypeStruct((ROWS, PER * HEAD), F32),
        jax.ShapeDtypeStruct((ROWS, STATE), F32),
    )
    far = pl.BlockSpec(memory_space=pltpu.MemorySpace.HBM)
    parts = pl.pallas_call(
        layer,
        name="layer",
        out_shape=outs,
        in_specs=[whole] * len(small) + [far] * len(STAGED),
        out_specs=[whole] * len(outs),
        scratch_shapes=[pltpu.VMEM(shape, dtype) for shape, dtype in SCRATCH.values()]
        + [
            pltpu.SemaphoreType.DMA((LEAVE,)),
            pltpu.SemaphoreType.DMA((ARRIVE,)),
            pltpu.SemaphoreType.DMA((len(STAGED),)),
        ],
        compiler_params=pltpu.CompilerParams(
            collective_id=0, has_side_effects=True, vmem_limit_bytes=VMEM_LIMIT
        ),
    )(*small, *(staged[name] for name in STAGED))
    state_shape = jax.ShapeDtypeStruct((ROWS, PER, HEAD, STATE), F32)
    result, conv_next, ssm_next = pl.pallas_call(
        finish,
        name="finish",
        out_shape=(*outs[:2], state_shape),
        in_specs=[whole] * len(outs) + [far],
        out_specs=[whole, whole, far],
        scratch_shapes=[pltpu.VMEM(state_shape.shape, F32)] * 2 + [pltpu.SemaphoreType.DMA((ROWS,))] * 2,
        compiler_params=pltpu.CompilerParams(vmem_limit_bytes=VMEM_LIMIT),
    )(*parts, ssm_state)
    return (result.T, ssm_next, conv_next.transpose(1, 0, 2)[:, :, None])


def solution(mesh):
    placed = (
        P(None, ("kv", "tp")),
        P("kv", "tp", None, None),
        P("kv", None, "tp", None),
        P(("kv", "tp")),
        P("kv", "tp"),
        P("kv", "tp"),
        P("tp", "kv"),
        P(("kv", "tp")),
        P("kv", "tp"),
        P("kv", "tp"),
        P("kv", "tp"),
        P("kv", "tp"),
        P("kv", "tp"),
        P(None, "tp", None),
        P("tp"),
        P("tp"),
        P("tp"),
        P("tp", "kv"),
        P(("kv", "tp")),
        P("kv", "tp"),
        P("kv", "tp"),
        P("tp", "kv"),
    )
    return jax.shard_map(
        on_device,
        mesh=mesh,
        in_specs=placed,
        out_specs=(P(None, ("kv", "tp")), P("kv", "tp", None, None), P("kv", None, "tp", None)),
        check_vma=False,
    )
```

time: 155 us -> 137 us (0.88)
  Pallas kernels: 148 us -> 136 us
  other arithmetic: 4.4 us -> 0 us
  local copies, waits for them, and re-layouts: 2.08 us -> 0 us
    pallas_call x1, Pallas kernels: 148 us -> 129 us  [on_device(): pl.pallas_call(layer, name='layer', out_shape=outs, in_specs=[whole] * le...]
    pallas_call x0 -> x1, Pallas kernels: none -> 6.75 us  [on_device(): pl.pallas_call(finish, name='finish', out_shape=(*outs[:2], state_shape),...]
    add x1 -> x0, other arithmetic: 4.4 us -> none  [on_device(): ssm_state * decay[:, :, None, None]]
where the time goes in v3:
time: 137 us
  Pallas kernels  136 us (99%)
    pallas_call x1, Pallas kernels, on_device(): pl.pallas_call(layer, name='layer', out_shape=outs, in_specs=[whole] * le...  129 us
    pallas_call x1, Pallas kernels, on_device(): pl.pallas_call(finish, name='finish', out_shape=(*outs[:2], state_shape),...  6.75 us

profile of v3, /device:TPU:1, one launch (start us, length us, event | category | flops | bytes accessed | tf_op | source)
XLA Modules:
  0.0 136.7 jit_solution(2730608400610937471)
XLA Ops:
  0.6 129.3 %layer.1 = (bf16[16,512]{1,0:T(8,128)(2,1)}, bf16[3,16,768]{2,1,0:T(8,128)(2,1)}, f32[16,512]{1,0:T(8,128)}, f32[16,512]{1,0:T(8,128)}, f32[16,128]{1,0:T(8,128)}) custom-call(bf16[16,512]{1,0:T(8,128)(2,1)} %bitcast.18, f32[1,16]{1,0:T(1,128)} %bitcast.21, f32[1,16]{1,0:T(1,128)} %bitcast.22, f32[1,16]{1,0:T(1,128)} %bitcast.23, bf16[8,128]{1,0:T(8,128)(2,1)} %bitcast.19, ...), custom_call_target="tpu_custom_call" | custom-call | tf_op jit(solution)/shard_map/layer/pallas_call | solution.py:680
  129.9 6.7 %finish.1 = (bf16[16,512]{1,0:T(8,128)(2,1)}, bf16[3,16,768]{2,1,0:T(8,128)(2,1)}, f32[16,8,64,128]{3,2,1,0:T(8,128)}) custom-call(bf16[16,512]{1,0:T(8,128)(2,1)} %get-tuple-element.11.stream_in, bf16[3,16,768]{2,1,0:T(8,128)(2,1)} %get-tuple-element.12.conv_in, f32[16,512]{1,0:T(8,128)} %get-tuple-element.13.kept, f32[16,512]{1,0:T(8,128)} %get-tuple-element.14.drive, ...), custom_call_target="tpu_custom_call" | custom-call | tf_op jit(solution)/shard_map/finish/pallas_call | solution.py:697

commit v4 on v3

--- a/solution.py
+++ b/solution.py
@@ -26,7 +26,8 @@
 
 class Wire:
     def __init__(self, sends, recvs):
-        self.sends, self.recvs, self.n_sends, self.n_recvs, self.pending = sends, recvs, 0, 0, []
+        self.sends, self.recvs, self.pending = sends, recvs, []
+        self.next = {False: [0, 0], True: [BULK_LEAVE, BULK_ARRIVE]}
         kv, self.tp = lax.axis_index("kv"), lax.axis_index("tp")
         self.kv = kv
         self.z, self.x = lax.div(kv, NX), lax.rem(kv, NX)
@@ -39,6 +40,13 @@
     def along_tp(self, d):
         return lax.rem(self.tp + d, NTP)
 
+    def start_over(self):
+        self.next[False] = [0, 0]
+
+    def take(self, bulk, kind):
+        self.next[bulk][kind] += 1
+        return self.next[bulk][kind] - 1
+
     def settle(self, keep=()):
         for copies in self.pending:
             if copies not in keep:
@@ -47,17 +55,15 @@
 
 
 class Copies:
-    def __init__(self, wire, every, pending=True):
-        self.wire, self.every, self.keys = wire, every, {}
-        self.sem = wire.sends.at[wire.n_sends]
-        wire.n_sends += 1
-        if pending:
+    def __init__(self, wire, every, bulk=False):
+        self.wire, self.every, self.bulk, self.keys = wire, every, bulk, {}
+        self.sem = wire.sends.at[wire.take(bulk, 0)]
+        if not bulk:
             wire.pending.append(self)
 
     def arrival(self, key):
         if key not in self.keys:
-            self.keys[key] = self.wire.n_recvs
-            self.wire.n_recvs += 1
+            self.keys[key] = self.wire.take(self.bulk, 1)
         return self.wire.recvs.at[self.keys[key]]
 
     def _copy(self, src, dst, kv, tp, key):
@@ -158,21 +164,39 @@
         dst[j * 128 : (j + 1) * 128, :] = src[:, j * 128 : (j + 1) * 128].T
 
 
-def send_gate_up(wire, plane, gate_t, up_t, both, part):
+def send_cut(wire, plane, turned, both, part, second):
     g = plane.g
     lanes = at_rows(g, FEAT, FEAT)
     start, size = PARTS[part]
-    out = []
-    for turned, at in ((gate_t, 2 * start), (up_t, 2 * start + size)):
-        copies = Copies(wire, both.at[at : at + size, 0 : (NZ - 1) * FEAT], False)
-
-        def cut(peer):
-            return pl.ds(pl.multiple_of(peer * CUT + start, OWN), size)
-
-        copies.to_g(plane, lambda peer: turned.at[cut(peer), :], both.at[at : at + size, lanes])
-        both[at : at + size, lanes] = turned[cut(g), :]
-        out.append(copies)
-    return out
+    at = 2 * start + second * size
+    copies = Copies(wire, both.at[at : at + size, 0 : (NZ - 1) * FEAT], True)
+
+    def cut(peer):
+        return pl.ds(pl.multiple_of(peer * CUT + start, OWN), size)
+
+    copies.to_g(plane, lambda peer: turned.at[cut(peer), :], both.at[at : at + size, lanes])
+    both[at : at + size, lanes] = turned[cut(g), :]
+    return copies
+
+
+class Hooks:
+    def after_first_sends(self):
+        pass
+
+    def after_forwards(self):
+        pass
+
+    def after_sums(self):
+        pass
+
+    def wait_weights(self, part):
+        pass
+
+    def after_hidden(self):
+        pass
+
+    def before_down(self):
+        pass
 
 
 def wait_all(sets):
@@ -182,7 +206,7 @@
 
 def send_down(wire, plane, down, parts):
     g = plane.g
-    copies = Copies(wire, parts.at[0 : NZ - 1], False)
+    copies = Copies(wire, parts.at[0 : NZ - 1], True)
     copies.to_g(plane, lambda peer: down.at[at_rows(peer, CUT, CUT), :], parts.at[g])
     parts[g] = down[at_rows(g, CUT, CUT), :]
     return copies
@@ -204,7 +228,7 @@
     return jnp.sum(jnp.where(same, square, 0.0), axis=1, keepdims=True)
 
 
-def gather_features(wire, plane, values, gain, feats, sq_g, sq_tp, after_first_sends):
+def gather_features(wire, plane, values, gain, feats, sq_g, sq_tp, after_first_sends, after_forwards):
     g, tp, c, sibling = plane.g, wire.tp, wire.c, wire.sibling
     wide = values.astype(F32)
     feats[g, tp] = (wide * as_column(gain[...])).astype(BF16)
@@ -229,6 +253,7 @@
     for d, peer in steps[1:]:
         to_group.arrived(feats.at[peer, tp], d)
         hand_on(d, peer)
+    after_forwards()
     squares_g.arrived(squares_g.every)
     sq_tp[tp] = jnp.sum(sq_g[...], axis=0)
     squares_tp = Copies(wire, sq_tp.at[0 : NTP - 1])
@@ -243,9 +268,11 @@
     return jnp.sum(sq_tp[...], axis=0)
 
 
-def channel_mixer(wire, plane, values, gain, s, after_first_sends, wait_weights, after_hidden, down_t):
+def channel_mixer(wire, plane, values, gain, s, hooks, down_t):
     g, h = plane.g, plane.h
-    squares = gather_features(wire, plane, values, gain, s["feats"], s["sq_g"], s["sq_tp"], after_first_sends)
+    squares = gather_features(
+        wire, plane, values, gain, s["feats"], s["sq_g"], s["sq_tp"], hooks.after_first_sends, hooks.after_forwards
+    )
     sq_h, sums, sums_h, hidden = s["sq_h"], s["sums"], s["sums_h"], s["hidden"]
     sq_h[h] = squares
     squares_h = Copies(wire, sq_h.at[0 : NX - 1])
@@ -253,7 +280,7 @@
     gathered = list(wire.pending)
     sums_out = []
     for part, (start, size) in enumerate(PARTS):
-        wait_weights(part)
+        hooks.wait_weights(part)
         rows = slice(2 * start, 2 * (start + size))
         sums[rows] = jnp.dot(
             s["both"][rows], s["feats"][...].reshape(DEPTH, SEQS), preferred_element_type=F32
@@ -262,6 +289,7 @@
         copies.to_h(plane, lambda peer: sums.at[rows, at_rows(peer, XS, XS)], sums_h.at[h, rows])
         sums_h[h, rows] = sums[rows, at_rows(h, XS, XS)]
         sums_out.append(copies)
+    hooks.after_sums()
     squares_h.arrived(squares_h.every)
     s["factor"][...] = lax.rsqrt(jnp.sum(sq_h[...], axis=0) / D + norm_epsilon)
     factor = s["factor"][:, at_rows(h, XS, XS)]
@@ -276,11 +304,12 @@
         out = Copies(wire, hidden.at[start : start + size, 0 : SEQS - XS])
         out.to_h(plane, lambda peer: here, here)
         hidden_out.append(out)
-    after_hidden()
+    hooks.after_hidden()
     for copies in gathered:
         copies.left()
     wire.pending = [copies for copies in wire.pending if copies not in gathered]
     wait_all(hidden_out)
+    hooks.before_down()
 
     c, y = wire.c, wire.y
     outs, other = s["outs"], s["other"]
@@ -349,6 +378,7 @@
     out_weight=((PER * HEAD, FEAT), BF16),
     state=((ROWS, PER, HEAD, STATE), F32),
     conv=((3, ROWS, PER * HEAD + 2 * STATE), BF16),
+    conv_next=((3, ROWS, PER * HEAD + 2 * STATE), BF16),
     mix_t=((NZ, MIX, FEAT), BF16),
     mix_in=((MIX, DEPTH), BF16),
     mix_feats=((NZ, NTP, OWN, SEQS), BF16),
@@ -376,7 +406,9 @@
     "conv",
     "out_weight",
 )
-LEAVE, ARRIVE = 56, 136
+BULK_LEAVE, BULK_ARRIVE = 22, 68
+LEAVE, ARRIVE = BULK_LEAVE + 11, BULK_ARRIVE + 11
+PIECES = 4
 VMEM_LIMIT = 58 * 1024 * 1024
 
 
@@ -453,14 +485,22 @@
     return (gated * scale * group_gain[...]).astype(BF16), (kept, drive, write_vec)
 
 
+def update_state(state, kept, drive, write_vec):
+    kept, drive = kept.T, drive.T
+    for b in range(ROWS):
+        flat = state[b].reshape(PER * HEAD, STATE)
+        new = flat * kept[:, b : b + 1] + drive[:, b : b + 1] * write_vec[b : b + 1]
+        state[b] = new.reshape(PER, HEAD, STATE)
+
+
 def layer(*refs):
     (stream, gain_1, gain_2, gain_3, step_in, conv_weight, step_bias, log_decay_rate, group_gain) = refs[:9]
     held = dict(zip(STAGED, refs[9 : 9 + len(STAGED)]))
     refs = refs[9 + len(STAGED) :]
-    result, conv_next, kept_out, drive_out, write_out = refs[:5]
-    refs = refs[5:]
+    result, conv_next, state_next = refs[:3]
+    refs = refs[3:]
     s = dict(zip(SCRATCH, refs))
-    sends, recvs, stage_sems = refs[len(SCRATCH) :]
+    sends, recvs, stage_sems, early_sems = refs[len(SCRATCH) :]
     wire = Wire(sends, recvs)
     plain, folded = Plane(wire, False), Plane(wire, True)
     z, x, kv, tp = wire.z, wire.x, wire.kv, wire.tp
@@ -478,42 +518,52 @@
     turn_columns(a["up"], a["up_t"])
     wait_greeting()
     sets = {}
-
-    def weights_out():
-        sets["first"] = [send_gate_up(wire, folded, a["gate_t"], a["up_t"], a["both"], part) for part in (0, 1)]
-        staging["a_down"].wait()
-        sets["down"] = send_down(wire, folded, a["down"], a["down_parts"])
-        for name in ("gate_in", "value_in", "write_in", "read_in"):
-            staging[name].wait()
-        turn_mixer(s, step_in)
-
-    def first_weights(part):
-        if part == 0:
-            staging["b_gate"].wait()
-            turn_columns(b["gate"], b["gate_t"])
-            staging["b_up"].wait()
-            turn_columns(b["up"], b["up_t"])
-        wait_all(sets["first"][part])
-
-    def after_first_hidden():
-        lanes = at_rows(folded.g, FEAT, FEAT)
-        sets["mix"] = Copies(wire, s["mix_in"].at[:, 0 : (NZ - 1) * FEAT], False)
-        sets["mix"].to_g(folded, lambda peer: s["mix_t"].at[peer], s["mix_in"].at[:, lanes])
-        s["mix_in"][:, lanes] = s["mix_t"][folded.g]
+    early = [
+        pltpu.make_async_copy(s["conv_next"], conv_next, early_sems.at[0]),
+        pltpu.make_async_copy(s["state"], state_next, early_sems.at[1]),
+    ]
+
+    class First(Hooks):
+        def after_first_sends(self):
+            sets["first"] = {0: [send_cut(wire, folded, a["gate_t"], a["both"], 0, 0)]}
+            sets["first"][0].append(send_cut(wire, folded, a["up_t"], a["both"], 0, 1))
+
+        def after_forwards(self):
+            sets["first"][1] = [send_cut(wire, folded, a["gate_t"], a["both"], 1, 0)]
+            sets["first"][1].append(send_cut(wire, folded, a["up_t"], a["both"], 1, 1))
+
+        def after_sums(self):
+            staging["a_down"].wait()
+            sets["down"] = send_down(wire, folded, a["down"], a["down_parts"])
+
+        def wait_weights(self, part):
+            wait_all(sets["first"][part])
+
+        def after_hidden(self):
+            for name in ("gate_in", "value_in", "write_in", "read_in"):
+                staging[name].wait()
+            turn_mixer(s, step_in)
+            s["mix_in"][:, at_rows(folded.g, FEAT, FEAT)] = s["mix_t"][folded.g]
+            wait_down(sets["down"], a["down_parts"], a["down_t"])
+
+        def before_down(self):
+            lanes = at_rows(folded.g, FEAT, FEAT)
+            sets["mix"] = Copies(wire, s["mix_in"].at[:, 0 : (NZ - 1) * FEAT], True)
+            sets["mix"].to_g(folded, lambda peer: s["mix_t"].at[peer], s["mix_in"].at[:, lanes])
+
+    branch = channel_mixer(wire, folded, stream[...], gain_1, a, First(), a["down_t"])
+    after = (stream[...].astype(F32) + 0.5 * branch).astype(BF16)
+
+    def next_down():
         staging["b_down"].wait()
         sets["next_down"] = send_down(wire, plain, b["down"], b["down_parts"])
-        wait_down(sets["down"], a["down_parts"], a["down_t"])
-
-    branch = channel_mixer(
-        wire, folded, stream[...], gain_1, a, weights_out, first_weights, after_first_hidden, a["down_t"]
-    )
-    after = (stream[...].astype(F32) + 0.5 * branch).astype(BF16)
-
-    def next_gate():
-        sets["second"] = [send_gate_up(wire, plain, b["gate_t"], b["up_t"], b["both"], 0)]
+        staging["b_gate"].wait()
+        turn_columns(b["gate"], b["gate_t"])
+        staging["b_up"].wait()
+        turn_columns(b["up"], b["up_t"])
 
     squares = gather_features(
-        wire, folded, after, gain_2, s["mix_feats"], s["mix_sq_g"], s["mix_sq_tp"], next_gate
+        wire, folded, after, gain_2, s["mix_feats"], s["mix_sq_g"], s["mix_sq_tp"], next_down, lambda: None
     )
     wait_all([sets["mix"]])
     part = jnp.dot(s["mix_in"][...], s["mix_feats"][...].reshape(DEPTH, SEQS), preferred_element_type=F32)
@@ -536,6 +586,7 @@
         peer = lax.rem(kv + d, NKV)
         row_copies.send(rows.at[peer], rows_in.at[kv], peer, tp)
 
+    sets["second"] = {0: [send_cut(wire, plain, b["gate_t"], b["both"], 0, 0)]}
     rows_in[kv] = rows[kv]
     wire.settle((row_copies,))
     wait_down(sets["next_down"], b["down_parts"], b["down_t"])
@@ -548,7 +599,7 @@
         step_bias,
         log_decay_rate,
         group_gain,
-        conv_next,
+        s["conv_next"],
         s["state"],
         lambda: staging["conv"].wait(),
     )
@@ -561,14 +612,16 @@
     for d in plain.near:
         to_z.send(own, own, plain.kv_at(plain.ahead(d), x), tp, d)
     to_x.to_h(plain, lambda peer: own, own)
-    sets["second"].append(send_gate_up(wire, plain, b["gate_t"], b["up_t"], b["both"], 1))
-    kept_out[...], drive_out[...], write_out[...] = change
+    early[0].start()
     staging["out_weight"].wait()
     wire.settle((to_z, to_x))
     for d in plain.near:
         block = mixed_all.at[plain.behind(d), x]
         to_z.arrived(block, d)
         to_x.to_h(plain, lambda peer: block, block)
+    sets["second"][0].append(send_cut(wire, plain, b["up_t"], b["both"], 0, 1))
+    sets["second"][1] = [send_cut(wire, plain, b["gate_t"], b["both"], 1, 0)]
+    sets["second"][1].append(send_cut(wire, plain, b["up_t"], b["both"], 1, 1))
     to_x.arrived(to_x.every)
     part = jnp.dot(mixed_all[...].reshape(SEQS, PER * HEAD), s["out_weight"][...], preferred_element_type=F32)
     out_t, out_in = s["out_t"], s["out_in"]
@@ -577,42 +630,46 @@
     to_tp.to_tp(lambda peer: out_t.at[peer], out_in.at[tp])
     out_in[tp] = out_t[tp]
     wire.settle((to_tp,))
+    update_state(s["state"], *change)
+    early[1].start()
     to_tp.arrived(to_tp.every)
     after = (after.astype(F32) + jnp.sum(out_in[...].astype(F32), axis=0)).astype(BF16)
 
-    def bulk_left():
-        for copies in [sets["down"], sets["mix"], sets["next_down"], *sum(sets["first"] + sets["second"], [])]:
-            copies.left()
-
-    branch = channel_mixer(
-        wire,
-        plain,
-        after,
-        gain_3,
-        b,
-        lambda: None,
-        lambda part: wait_all(sets["second"][part]),
-        bulk_left,
-        b["down_t"],
-    )
+    assert wire.next[False] == [BULK_LEAVE, BULK_ARRIVE], wire.next
+
+    class Second(Hooks):
+        def wait_weights(self, part):
+            wait_all(sets["second"][part])
+
+        def after_hidden(self):
+            gates_ups = [copies for part in (0, 1) for name in ("first", "second") for copies in sets[name][part]]
+            for copies in [sets["down"], sets["mix"], sets["next_down"], *gates_ups]:
+                copies.left()
+            for copy in early:
+                copy.wait()
+
+    wire.start_over()
+    branch = channel_mixer(wire, plain, after, gain_3, b, Second(), b["down_t"])
+    assert wire.next[True] == [LEAVE, ARRIVE]
     result[...] = (after.astype(F32) + 0.5 * branch).astype(BF16)
     wire.settle()
 
 
-def finish(stream_in, conv_in, kept, drive, write_vec, state, result, conv_next, state_next, held, done, reads, writes):
-    into = [pltpu.make_async_copy(state.at[b], held.at[b], reads.at[b]) for b in range(ROWS)]
-    out = [pltpu.make_async_copy(done.at[b], state_next.at[b], writes.at[b]) for b in range(ROWS)]
+def finish(*refs):
+    far_in, far_out, near = refs[:3], refs[3:6], refs[6:9]
+    reads, writes = refs[9:]
+    piece = ROWS // PIECES
+    pairs = [(far_in[i], near[i], far_out[i]) for i in (0, 1)]
+    for i in range(PIECES):
+        at = pl.ds(i * piece, piece)
+        pairs.append(tuple(ref.at[at] for ref in (far_in[2], near[2], far_out[2])))
+    into = [pltpu.make_async_copy(a, b, reads.at[i]) for i, (a, b, _) in enumerate(pairs)]
+    out = [pltpu.make_async_copy(b, c, writes.at[i]) for i, (_, b, c) in enumerate(pairs)]
     for copy in into:
         copy.start()
-    kept_t, drive_t = kept[...].T, drive[...].T
-    result[...] = stream_in[...]
-    conv_next[...] = conv_in[...]
-    for b in range(ROWS):
-        into[b].wait()
-        flat = held[b].reshape(PER * HEAD, STATE)
-        new = flat * kept_t[:, b : b + 1] + drive_t[:, b : b + 1] * write_vec[b : b + 1]
-        done[b] = new.reshape(PER, HEAD, STATE)
-        out[b].start()
+    for first, second in zip(into, out):
+        first.wait()
+        second.start()
     for copy in out:
         copy.wait()
 
@@ -669,12 +726,11 @@
     )
     whole = pl.BlockSpec(memory_space=pltpu.VMEM)
     channels = PER * HEAD + 2 * STATE
+    channels = PER * HEAD + 2 * STATE
     outs = (
         jax.ShapeDtypeStruct((OWN, SEQS), BF16),
         jax.ShapeDtypeStruct((3, ROWS, channels), BF16),
-        jax.ShapeDtypeStruct((ROWS, PER * HEAD), F32),
-        jax.ShapeDtypeStruct((ROWS, PER * HEAD), F32),
-        jax.ShapeDtypeStruct((ROWS, STATE), F32),
+        jax.ShapeDtypeStruct((ROWS, PER, HEAD, STATE), F32),
     )
     far = pl.BlockSpec(memory_space=pltpu.MemorySpace.HBM)
     parts = pl.pallas_call(
@@ -682,27 +738,28 @@
         name="layer",
         out_shape=outs,
         in_specs=[whole] * len(small) + [far] * len(STAGED),
-        out_specs=[whole] * len(outs),
+        out_specs=[whole] + [far] * (len(outs) - 1),
         scratch_shapes=[pltpu.VMEM(shape, dtype) for shape, dtype in SCRATCH.values()]
         + [
             pltpu.SemaphoreType.DMA((LEAVE,)),
             pltpu.SemaphoreType.DMA((ARRIVE,)),
             pltpu.SemaphoreType.DMA((len(STAGED),)),
+            pltpu.SemaphoreType.DMA((len(outs) - 1,)),
         ],
         compiler_params=pltpu.CompilerParams(
             collective_id=0, has_side_effects=True, vmem_limit_bytes=VMEM_LIMIT
         ),
     )(*small, *(staged[name] for name in STAGED))
-    state_shape = jax.ShapeDtypeStruct((ROWS, PER, HEAD, STATE), F32)
     result, conv_next, ssm_next = pl.pallas_call(
         finish,
         name="finish",
-        out_shape=(*outs[:2], state_shape),
-        in_specs=[whole] * len(outs) + [far],
-        out_specs=[whole, whole, far],
-        scratch_shapes=[pltpu.VMEM(state_shape.shape, F32)] * 2 + [pltpu.SemaphoreType.DMA((ROWS,))] * 2,
+        out_shape=outs,
+        in_specs=[far] * len(outs),
+        out_specs=[far] * len(outs),
+        scratch_shapes=[pltpu.VMEM(out.shape, out.dtype) for out in outs]
+        + [pltpu.SemaphoreType.DMA((PIECES + 2,))] * 2,
         compiler_params=pltpu.CompilerParams(vmem_limit_bytes=VMEM_LIMIT),
-    )(*parts, ssm_state)
+    )(*parts)
     return (result.T, ssm_next, conv_next.transpose(1, 0, 2)[:, :, None])
 
 

time: 137 us -> 133 us (0.971)
  Pallas kernels: 136 us -> 132 us
    pallas_call x1, Pallas kernels: 6.75 us -> 3.46 us  [on_device(): pl.pallas_call(finish, name='finish', out_shape=outs, in_specs=[far] * le...]
where the time goes in v4:
time: 133 us
  Pallas kernels  132 us (99%)
    pallas_call x1, Pallas kernels, on_device(): pl.pallas_call(layer, name='layer', out_shape=outs, in_specs=[whole] * le...  129 us
    pallas_call x1, Pallas kernels, on_device(): pl.pallas_call(finish, name='finish', out_shape=outs, in_specs=[far] * le...  3.46 us

profile of v4, /device:TPU:1, one launch (start us, length us, event | category | flops | bytes accessed | tf_op | source)
XLA Modules:
  0.0 133.1 jit_solution(4314598771835515853)
XLA Ops:
  0.6 129.0 %layer.1 = (bf16[16,512]{1,0:T(8,128)(2,1)}, bf16[3,16,768]{2,1,0:T(8,128)(2,1)}, f32[16,8,64,128]{3,2,1,0:T(8,128)}) custom-call(bf16[16,512]{1,0:T(8,128)(2,1)} %bitcast.18, f32[1,16]{1,0:T(1,128)} %bitcast.21, f32[1,16]{1,0:T(1,128)} %bitcast.22, f32[1,16]{1,0:T(1,128)} %bitcast.23, bf16[8,128]{1,0:T(8,128)(2,1)} %bitcast.19, f32[4,1,768]{2,1,0:T(1,128)} %refs_5_.1, ...), custom_call_target="tpu_custom_call" | custom-call | tf_op jit(solution)/shard_map/layer/pallas_call | solution.py:736
  129.6 3.5 %finish.1 = (bf16[16,512]{1,0:T(8,128)(2,1)}, bf16[3,16,768]{2,1,0:T(8,128)(2,1)}, f32[16,8,64,128]{3,2,1,0:T(8,128)}) custom-call(bf16[16,512]{1,0:T(8,128)(2,1)} %get-tuple-element.9.refs_0_, bf16[3,16,768]{2,1,0:T(8,128)(2,1)} %get-tuple-element.10.refs_1_, f32[16,8,64,128]{3,2,1,0:T(8,128)} %get-tuple-element.11.refs_2_), custom_call_target="tpu_custom_call" | custom-call | tf_op jit(solution)/shard_map/finish/pallas_call | solution.py:753

commit v5 on v4

--- a/solution.py
+++ b/solution.py
@@ -234,8 +234,6 @@
     feats[g, tp] = (wide * as_column(gain[...])).astype(BF16)
     own = feats.at[g, tp]
     to_group = Copies(wire, feats.at[0, 0 : NZ - 1])
-    for d in plane.near:
-        to_group.send(own, own, plane.kv_at(plane.ahead(d), plane.h), tp, d)
     along = Copies(wire, feats.at[0 : NY - 1])
     across = Copies(wire, feats.at[0:NY])
 
@@ -245,6 +243,8 @@
         across.send(block, block, wire.kv, sibling)
 
     hand_on(0, g)
+    for d in plane.near:
+        to_group.send(own, own, plane.kv_at(plane.ahead(d), plane.h), tp, d)
     sq_g[g] = jnp.sum(wide * wide, axis=0, keepdims=True)
     squares_g = Copies(wire, sq_g.at[0 : NZ - 1])
     squares_g.to_g(plane, lambda peer: sq_g.at[g], sq_g.at[g])
@@ -517,7 +517,16 @@
     staging["a_up"].wait()
     turn_columns(a["up"], a["up_t"])
     wait_greeting()
-    sets = {}
+    sets = {"second": {0: [], 1: []}}
+
+    def second(part, which):
+        turned = b["up_t"] if which else b["gate_t"]
+        sets["second"][part].append(send_cut(wire, plain, turned, b["both"], part, which))
+
+    def second_down():
+        staging["b_down"].wait()
+        sets["next_down"] = send_down(wire, plain, b["down"], b["down_parts"])
+
     early = [
         pltpu.make_async_copy(s["conv_next"], conv_next, early_sems.at[0]),
         pltpu.make_async_copy(s["state"], state_next, early_sems.at[1]),
@@ -525,16 +534,16 @@
 
     class First(Hooks):
         def after_first_sends(self):
-            sets["first"] = {0: [send_cut(wire, folded, a["gate_t"], a["both"], 0, 0)]}
-            sets["first"][0].append(send_cut(wire, folded, a["up_t"], a["both"], 0, 1))
+            sets["first"] = {0: [send_cut(wire, plain, a["gate_t"], a["both"], 0, 0)]}
+            sets["first"][0].append(send_cut(wire, plain, a["up_t"], a["both"], 0, 1))
 
         def after_forwards(self):
-            sets["first"][1] = [send_cut(wire, folded, a["gate_t"], a["both"], 1, 0)]
-            sets["first"][1].append(send_cut(wire, folded, a["up_t"], a["both"], 1, 1))
+            sets["first"][1] = [send_cut(wire, plain, a["gate_t"], a["both"], 1, 0)]
+            sets["first"][1].append(send_cut(wire, plain, a["up_t"], a["both"], 1, 1))
 
         def after_sums(self):
             staging["a_down"].wait()
-            sets["down"] = send_down(wire, folded, a["down"], a["down_parts"])
+            sets["down"] = send_down(wire, plain, a["down"], a["down_parts"])
 
         def wait_weights(self, part):
             wait_all(sets["first"][part])
@@ -543,6 +552,10 @@
             for name in ("gate_in", "value_in", "write_in", "read_in"):
                 staging[name].wait()
             turn_mixer(s, step_in)
+            for name in ("b_gate", "b_up"):
+                staging[name].wait()
+            turn_columns(b["gate"], b["gate_t"])
+            turn_columns(b["up"], b["up_t"])
             s["mix_in"][:, at_rows(folded.g, FEAT, FEAT)] = s["mix_t"][folded.g]
             wait_down(sets["down"], a["down_parts"], a["down_t"])
 
@@ -551,19 +564,16 @@
             sets["mix"] = Copies(wire, s["mix_in"].at[:, 0 : (NZ - 1) * FEAT], True)
             sets["mix"].to_g(folded, lambda peer: s["mix_t"].at[peer], s["mix_in"].at[:, lanes])
 
-    branch = channel_mixer(wire, folded, stream[...], gain_1, a, First(), a["down_t"])
+    branch = channel_mixer(wire, plain, stream[...], gain_1, a, First(), a["down_t"])
     after = (stream[...].astype(F32) + 0.5 * branch).astype(BF16)
 
-    def next_down():
-        staging["b_down"].wait()
-        sets["next_down"] = send_down(wire, plain, b["down"], b["down_parts"])
-        staging["b_gate"].wait()
-        turn_columns(b["gate"], b["gate_t"])
-        staging["b_up"].wait()
-        turn_columns(b["up"], b["up_t"])
+    def early_second():
+        second(0, 0)
+        second(0, 1)
+        second(1, 0)
 
     squares = gather_features(
-        wire, folded, after, gain_2, s["mix_feats"], s["mix_sq_g"], s["mix_sq_tp"], next_down, lambda: None
+        wire, folded, after, gain_2, s["mix_feats"], s["mix_sq_g"], s["mix_sq_tp"], early_second, lambda: None
     )
     wait_all([sets["mix"]])
     part = jnp.dot(s["mix_in"][...], s["mix_feats"][...].reshape(DEPTH, SEQS), preferred_element_type=F32)
@@ -579,17 +589,12 @@
     rows[...] = turned[...].T.astype(BF16).reshape(NKV, ROWS, WIDE)
 
     row_copies = Copies(wire, rows.at[0 : NKV - 1])
-    row_copies.arrival(0)
-
-    @pl.loop(1, NKV)
-    def _(d):
-        peer = lax.rem(kv + d, NKV)
+    offsets = [(dz, dx) for dz in range(NZ) for dx in range(NX) if dz or dx]
+    for dz, dx in sorted(offsets, key=lambda o: -min(o[0], NZ - o[0]) - min(o[1], NX - o[1])):
+        peer = lax.rem(z + dz, NZ) * NX + lax.rem(x + dx, NX)
         row_copies.send(rows.at[peer], rows_in.at[kv], peer, tp)
-
-    sets["second"] = {0: [send_cut(wire, plain, b["gate_t"], b["both"], 0, 0)]}
     rows_in[kv] = rows[kv]
     wire.settle((row_copies,))
-    wait_down(sets["next_down"], b["down_parts"], b["down_t"])
     staging["state"].wait()
     row_copies.arrived(rows_in.at[0 : NKV - 1])
     mixed, change = state_step(
@@ -619,9 +624,8 @@
         block = mixed_all.at[plain.behind(d), x]
         to_z.arrived(block, d)
         to_x.to_h(plain, lambda peer: block, block)
-    sets["second"][0].append(send_cut(wire, plain, b["up_t"], b["both"], 0, 1))
-    sets["second"][1] = [send_cut(wire, plain, b["gate_t"], b["both"], 1, 0)]
-    sets["second"][1].append(send_cut(wire, plain, b["up_t"], b["both"], 1, 1))
+    second(1, 1)
+    second_down()
     to_x.arrived(to_x.every)
     part = jnp.dot(mixed_all[...].reshape(SEQS, PER * HEAD), s["out_weight"][...], preferred_element_type=F32)
     out_t, out_in = s["out_t"], s["out_in"]
@@ -642,6 +646,7 @@
             wait_all(sets["second"][part])
 
         def after_hidden(self):
+            wait_down(sets["next_down"], b["down_parts"], b["down_t"])
             gates_ups = [copies for part in (0, 1) for name in ("first", "second") for copies in sets[name][part]]
             for copies in [sets["down"], sets["mix"], sets["next_down"], *gates_ups]:
                 copies.left()

time: 133 us -> 130 us (0.977)
  Pallas kernels: 132 us -> 129 us
    pallas_call x1, Pallas kernels: 129 us -> 125 us  [on_device(): pl.pallas_call(layer, name='layer', out_shape=outs, in_specs=[whole] * le...]
where the time goes in v5:
time: 130 us; the launch traced here: 129 us
  Pallas kernels  129 us (99%)
    pallas_call x1, Pallas kernels, on_device(): pl.pallas_call(layer, name='layer', out_shape=outs, in_specs=[whole] * le...  125 us
    pallas_call x1, Pallas kernels, on_device(): pl.pallas_call(finish, name='finish', out_shape=outs, in_specs=[far] * le...  3.46 us

profile of v5, /device:TPU:1, one launch (start us, length us, event | category | flops | bytes accessed | tf_op | source)
XLA Modules:
  0.0 129.3 jit_solution(1816879170015645103)
XLA Ops:
  0.6 125.2 %layer.1 = (bf16[16,512]{1,0:T(8,128)(2,1)}, bf16[3,16,768]{2,1,0:T(8,128)(2,1)}, f32[16,8,64,128]{3,2,1,0:T(8,128)}) custom-call(bf16[16,512]{1,0:T(8,128)(2,1)} %bitcast.18, f32[1,16]{1,0:T(1,128)} %bitcast.21, f32[1,16]{1,0:T(1,128)} %bitcast.22, f32[1,16]{1,0:T(1,128)} %bitcast.23, bf16[8,128]{1,0:T(8,128)(2,1)} %bitcast.19, f32[4,1,768]{2,1,0:T(1,128)} %refs_5_.1, ...), custom_call_target="tpu_custom_call" | custom-call | tf_op jit(solution)/shard_map/layer/pallas_call | solution.py:741
  125.8 3.5 %finish.1 = (bf16[16,512]{1,0:T(8,128)(2,1)}, bf16[3,16,768]{2,1,0:T(8,128)(2,1)}, f32[16,8,64,128]{3,2,1,0:T(8,128)}) custom-call(bf16[16,512]{1,0:T(8,128)(2,1)} %get-tuple-element.9.refs_0_, bf16[3,16,768]{2,1,0:T(8,128)(2,1)} %get-tuple-element.10.refs_1_, f32[16,8,64,128]{3,2,1,0:T(8,128)} %get-tuple-element.11.refs_2_), custom_call_target="tpu_custom_call" | custom-call | tf_op jit(solution)/shard_map/finish/pallas_call | solution.py:758

commit v6 on v5

--- a/solution.py
+++ b/solution.py
@@ -149,10 +149,9 @@
     for d in range(1, NX):
         x = lax.rem(wire.x + d, NX)
         tell(wire.z * NX + x, wire.tp)
-        tell((wire.z + 1 - 2 * lax.rem(wire.z, 2)) * NX + x, wire.tp)
     for d in range(1, NTP):
         tell(wire.kv, wire.along_tp(d))
-    return lambda: pl.semaphore_wait(barrier, NZ - 1 + 2 * (NX - 1) + NTP - 1)
+    return lambda: pl.semaphore_wait(barrier, NZ - 1 + NX - 1 + NTP - 1)
 
 
 def at_rows(start, size, step):
@@ -546,16 +545,17 @@
             sets["down"] = send_down(wire, plain, a["down"], a["down_parts"])
 
         def wait_weights(self, part):
+            if part == 0:
+                for name in ("b_gate", "b_up"):
+                    staging[name].wait()
+                turn_columns(b["gate"], b["gate_t"])
+                turn_columns(b["up"], b["up_t"])
             wait_all(sets["first"][part])
 
         def after_hidden(self):
             for name in ("gate_in", "value_in", "write_in", "read_in"):
                 staging[name].wait()
             turn_mixer(s, step_in)
-            for name in ("b_gate", "b_up"):
-                staging[name].wait()
-            turn_columns(b["gate"], b["gate_t"])
-            turn_columns(b["up"], b["up_t"])
             s["mix_in"][:, at_rows(folded.g, FEAT, FEAT)] = s["mix_t"][folded.g]
             wait_down(sets["down"], a["down_parts"], a["down_t"])
 

time: 130 us -> 130 us (level)
  no operation moved by 1% of the time
where the time goes in v6:
time: 130 us; the launch traced here: 129 us
  Pallas kernels  129 us (99%)
    pallas_call x1, Pallas kernels, on_device(): pl.pallas_call(layer, name='layer', out_shape=outs, in_specs=[whole] * le...  125 us
    pallas_call x1, Pallas kernels, on_device(): pl.pallas_call(finish, name='finish', out_shape=outs, in_specs=[far] * le...  3.46 us

profile of v6, /device:TPU:1, one launch (start us, length us, event | category | flops | bytes accessed | tf_op | source)
XLA Modules:
  0.0 129.3 jit_solution(13557087913329790454)
XLA Ops:
  0.6 125.2 %layer.1 = (bf16[16,512]{1,0:T(8,128)(2,1)}, bf16[3,16,768]{2,1,0:T(8,128)(2,1)}, f32[16,8,64,128]{3,2,1,0:T(8,128)}) custom-call(bf16[16,512]{1,0:T(8,128)(2,1)} %bitcast.18, f32[1,16]{1,0:T(1,128)} %bitcast.21, f32[1,16]{1,0:T(1,128)} %bitcast.22, f32[1,16]{1,0:T(1,128)} %bitcast.23, bf16[8,128]{1,0:T(8,128)(2,1)} %bitcast.19, f32[4,1,768]{2,1,0:T(1,128)} %refs_5_.1, ...), custom_call_target="tpu_custom_call" | custom-call | tf_op jit(solution)/shard_map/layer/pallas_call | solution.py:741
  125.9 3.5 %finish.1 = (bf16[16,512]{1,0:T(8,128)(2,1)}, bf16[3,16,768]{2,1,0:T(8,128)(2,1)}, f32[16,8,64,128]{3,2,1,0:T(8,128)}) custom-call(bf16[16,512]{1,0:T(8,128)(2,1)} %get-tuple-element.9.refs_0_, bf16[3,16,768]{2,1,0:T(8,128)(2,1)} %get-tuple-element.10.refs_1_, f32[16,8,64,128]{3,2,1,0:T(8,128)} %get-tuple-element.11.refs_2_), custom_call_target="tpu_custom_call" | custom-call | tf_op jit(solution)/shard_map/finish/pallas_call | solution.py:758
